TPU v7x, 32 devices: a whole 2x2x4 slice. The times are simulated.
32 devices in a mesh: sp: 8 (over z, x), tp: 4 (over y, core).
Axes of the slice: x: 2, y: 2, z: 4, core: 2. Of those that a mesh axis runs over, the one named last changes fastest.
Arguments:
- tokens: bfloat16 [4096, 2048], P(('sp', 'tp')), may hold values from -6 to 6
- norm_gain: float32 [2048], replicated, may hold values from 0.1 to 1.9
- rec_query: bfloat16 [2048, 1024], P(None, 'tp'), may hold values from -0.125 to 0.125
- fwd_gate: bfloat16 [2048, 1024], P(None, 'tp'), may hold values from -0.125 to 0.125
- bwd_gate: bfloat16 [2048, 1024], P(None, 'tp'), may hold values from -0.125 to 0.125
- rec_value: bfloat16 [2048, 1024], P(None, 'tp'), may hold values from -0.125 to 0.125
- gate_leak: float32 [2, 1024], P(None, 'tp'), may hold values from 0 to 0.08, as said below
- log_decay: float32 [2, 4096, 8], P(None, 'sp', 'tp'), may hold values from -2.2 to 0, as said below
- rec_gain: float32 [128], replicated, may hold values from 0.1 to 1.9
- att_query: bfloat16 [2048, 1024], P(None, 'tp'), as said below
- att_key: bfloat16 [2048, 1024], P(None, 'tp')
- att_value: bfloat16 [2048, 1024], P(None, 'tp'), may hold values from -0.125 to 0.125
- lambdas: float32 [8], P('tp'), may hold values from 0.3 to 0.8
- att_gain: float32 [128], replicated, may hold values from 0.1 to 1.9
- out_rec: bfloat16 [1024, 2048], replicated, may hold values from -0.125 to 0.125
- out_att: bfloat16 [1024, 2048], replicated, may hold values from -0.125 to 0.125
Outputs:
- layer_out: bfloat16 [4096, 2048], P(('sp', 'tp'))
Inputs may be any that keep to these rules, and one draw needn't show every extreme that they name: `gate_leak`: positive, by direction and channel. `log_decay`: never positive. `att_query`: entries of order 2048 to the power -1/2.
All inputs are finite; a program needn't handle non-finite values.
Results may differ from a plain program's by a relative error of at most 0.011.
Values may be sent and summed in bfloat16 or wider, within the bound.
A program may use at most 128 MiB of HBM per device.

v0:
```python
import math

import jax
import jax.numpy as jnp
from jax import lax
from jax.sharding import PartitionSpec as P

HK = 128
HV = 128
AK = 64
AV = 128
BLOCK = 64


EPS = 1e-06
THETA = 500000.0
HIGHEST = lax.Precision.HIGHEST


def passed_along(value, axis, by):
    size = lax.axis_size(axis)
    return lax.ppermute(value, axis, [(i, (i + by) % size) for i in range(size)])


def passed_along_2(block, axis, distance):
    devices = range(lax.axis_size(axis))
    route = [(i - distance, i) for i in devices if i - distance in devices]
    return lax.ppermute(block, axis, route)


def rms_scale(values, gain):
    return values * lax.rsqrt(jnp.mean(values * values, axis=-1, keepdims=True) + EPS) * gain


def block_recurrence(queries, keys_in, values, log_forget):
    head_count, length, key_width = queries.shape
    value_width = values.shape[-1]
    block_count = length // BLOCK
    block_shape = (head_count, block_count, BLOCK, key_width)
    query_blocks = queries.reshape(block_shape)
    key_blocks = keys_in.reshape(block_shape)
    value_blocks = values.reshape(head_count, block_count, BLOCK, value_width)
    cumulative = jnp.cumsum(log_forget.reshape(block_shape), axis=2)
    middle = cumulative[:, :, BLOCK // 2 - 1 : BLOCK // 2]
    block_last = cumulative[:, :, BLOCK - 1 :]
    scores = jnp.einsum(
        "hntd,hnsd->hnts",
        query_blocks * jnp.exp(cumulative - middle),
        key_blocks * jnp.exp(middle - cumulative),
        precision=HIGHEST,
    )
    causal_mask = jnp.arange(BLOCK)[:, None] >= jnp.arange(BLOCK)[None, :]
    scores = jnp.where(causal_mask, scores, 0.0)
    within_out = jnp.einsum("hnts,hnsv->hntv", scores, value_blocks, precision=HIGHEST)
    per_block_state = jnp.einsum(
        "hnsd,hnsv->hndv",
        key_blocks * jnp.exp(block_last - cumulative),
        value_blocks,
        precision=HIGHEST,
    )
    block_decay = jnp.exp(block_last[:, :, 0])

    def advance(running, inputs_now):
        factor, added_state = inputs_now
        return (factor[..., None] * running + added_state, running)

    initial = jnp.zeros((head_count, key_width, value_width), jnp.float32)
    end_state, before = lax.scan(
        advance, initial, (jnp.moveaxis(block_decay, 1, 0), jnp.moveaxis(per_block_state, 1, 0))
    )
    before = jnp.moveaxis(before, 0, 1)
    carried = jnp.einsum(
        "hntd,hndv->hntv", query_blocks * jnp.exp(cumulative), before, precision=HIGHEST
    )
    return ((within_out + carried).reshape(head_count, length, value_width), end_state, cumulative)


def local_direction(queries, keys_in, values, log_forget):
    outputs, end_state, cumulative = block_recurrence(queries, keys_in, values, log_forget)
    head_count, length, key_width = queries.shape
    block_totals = cumulative[:, :, BLOCK - 1]
    before_block = jnp.cumsum(block_totals, axis=1) - block_totals
    within = (cumulative + before_block[:, :, None]).reshape(head_count, length, key_width)
    return (outputs, jnp.exp(jnp.sum(block_totals, axis=1)), end_state, queries * jnp.exp(within))


def rotate(vectors, positions):
    half_width = AK // 2
    frequency = THETA ** (-(jnp.arange(half_width, dtype=jnp.float32) * 2.0 / AK))
    angles = positions[:, None] * frequency[None, :]
    cosine = jnp.cos(angles)[:, None, None, :]
    sines = jnp.sin(angles)[:, None, None, :]
    first_half = vectors[..., :half_width]
    second = vectors[..., half_width:]
    return jnp.concatenate(
        [first_half * cosine - second * sines, second * cosine + first_half * sines], axis=-1
    )


def attend(carry, queries, key_rows, value_rows):
    head_count = queries.shape[1]
    row_count = key_rows.shape[0]
    span_rows = math.gcd(row_count, 1024)
    key_blocks = key_rows.reshape(row_count // span_rows, span_rows, head_count, 2, AK)
    value_blocks = value_rows.reshape(row_count // span_rows, span_rows, head_count, AV)

    def absorb(running, inputs_now):
        peak_values, totals, summed = running
        key_block, value_block = inputs_now
        scores = jnp.einsum(
            "qhmd,khmd->hmqk", queries, key_block, preferred_element_type=jnp.float32
        )
        raised = jnp.maximum(peak_values, jnp.max(scores, axis=-1))
        shrink = jnp.exp(peak_values - raised)
        weights_raw = jnp.exp(scores - raised[..., None])
        totals = totals * shrink + jnp.sum(weights_raw, axis=-1)
        summed = summed * shrink[..., None] + jnp.einsum(
            "hmqk,khv->hmqv",
            weights_raw.astype(jnp.bfloat16),
            value_block,
            preferred_element_type=jnp.float32,
        )
        return ((raised, totals, summed), None)

    running, unused = lax.scan(absorb, carry, (key_blocks, value_blocks))
    return running


def on_device(
    tokens,
    norm_gain,
    rec_query,
    fwd_gate,
    bwd_gate,
    rec_value,
    gate_leak,
    log_decay,
    rec_gain,
    att_query,
    att_key,
    att_value,
    lambdas,
    att_gain,
    out_rec,
    out_att,
):
    normed = rms_scale(tokens.astype(jnp.float32), norm_gain).astype(jnp.bfloat16)
    weights_all = (rec_query, fwd_gate, bwd_gate, rec_value, att_query, att_key, att_value)
    joined = jnp.concatenate(weights_all, axis=1)
    projected = jnp.dot(
        lax.all_gather(normed, "tp", axis=0, tiled=True), joined, preferred_element_type=jnp.float32
    ).astype(jnp.bfloat16)
    length = projected.shape[0]
    columns = []
    column_start = 0
    for weight in weights_all:
        columns.append(projected[:, column_start : column_start + weight.shape[1]])
        column_start = column_start + weight.shape[1]
    query_raw, fwd_raw, bwd_raw, value_raw, att_query_raw, att_key_raw, att_value_raw = columns

    def split_heads(table, width):
        return table.astype(jnp.float32).reshape(length, -1, width).transpose(1, 0, 2)

    queries = jax.nn.silu(split_heads(query_raw, HK))
    values = split_heads(value_raw, HV)
    rec_heads = queries.shape[0]
    key_fwd = gate_leak[0].reshape(rec_heads, 1, HK) * jax.nn.sigmoid(-split_heads(fwd_raw, HK))
    key_bwd = gate_leak[1].reshape(rec_heads, 1, HK) * jax.nn.sigmoid(-split_heads(bwd_raw, HK))
    log_fwd = jnp.log1p(-key_fwd) + log_decay[0].T[:, :, None]
    log_bwd = jnp.log1p(-key_bwd) + log_decay[1].T[:, :, None]
    out_fwd, decay_fwd, ending_fwd, read_fwd = local_direction(queries, key_fwd, values, log_fwd)
    out_back, decay_bwd, ending_bwd, read_bwd = local_direction(
        jnp.flip(queries, 1), jnp.flip(key_bwd, 1), jnp.flip(values, 1), jnp.flip(log_bwd, 1)
    )
    positions = (lax.axis_index("sp") * length + jnp.arange(length, dtype=jnp.int32)).astype(
        jnp.float32
    )
    att_queries = (
        rotate(att_query_raw.astype(jnp.float32).reshape(length, -1, 2, AK), positions)
        * AK ** (-0.5)
    ).astype(jnp.bfloat16)
    att_keys = (
        rotate(att_key_raw.astype(jnp.float32).reshape(length, -1, 2, AK), positions)
        .astype(jnp.bfloat16)
        .reshape(length, -1)
    )
    att_heads = att_queries.shape[1]
    initial = (
        jnp.full((att_heads, 2, length), -jnp.inf, jnp.float32),
        jnp.zeros((att_heads, 2, length), jnp.float32),
        jnp.zeros((att_heads, 2, length, AV), jnp.float32),
    )
    turn_count = lax.axis_size("sp") - 1

    def relay_turn(turn_index, carried):
        running, key_rows, value_rows, inbound_fwd, inbound_bwd = carried
        key_rows, value_rows = passed_along((key_rows, value_rows), "sp", 1)
        inbound_fwd = passed_along_2(
            (decay_fwd[..., None] * inbound_fwd + ending_fwd).astype(jnp.bfloat16), "sp", 1
        ).astype(jnp.float32)
        inbound_bwd = passed_along_2(
            (decay_bwd[..., None] * inbound_bwd + ending_bwd).astype(jnp.bfloat16), "sp", -1
        ).astype(jnp.float32)
        running = attend(running, att_queries, key_rows, value_rows)
        return (running, key_rows, value_rows, inbound_fwd, inbound_bwd)

    start_state = (
        attend(initial, att_queries, att_keys, att_value_raw),
        att_keys,
        att_value_raw,
        jnp.zeros_like(ending_fwd),
        jnp.zeros_like(ending_bwd),
    )
    running, unused_keys, unused_values, entry_fwd, entry_bwd = lax.fori_loop(
        0, turn_count, relay_turn, start_state
    )
    out_fwd = out_fwd + jnp.einsum("hld,hdv->hlv", read_fwd, entry_fwd, precision=HIGHEST)
    out_back = out_back + jnp.einsum("hld,hdv->hlv", read_bwd, entry_bwd, precision=HIGHEST)
    rec_rows = rms_scale(out_fwd + jnp.flip(out_back, 1), rec_gain)
    rec_rows = rec_rows.transpose(1, 0, 2).reshape(length, -1).astype(jnp.bfloat16)
    peak_values, totals, summed = running
    ratio = summed / totals[..., None]
    mixed_heads = ratio[:, 0] - lambdas[:, None, None] * ratio[:, 1]
    att_rows = (
        rms_scale(mixed_heads, att_gain).transpose(1, 0, 2).reshape(length, -1).astype(jnp.bfloat16)
    )
    rec_all, att_all = (
        lax.all_to_all(rec_rows, "tp", split_axis=0, concat_axis=1, tiled=True),
        lax.all_to_all(att_rows, "tp", split_axis=0, concat_axis=1, tiled=True),
    )
    projected_out = jnp.dot(rec_all, out_rec, preferred_element_type=jnp.float32) + jnp.dot(
        att_all, out_att, preferred_element_type=jnp.float32
    )
    return projected_out.astype(jnp.bfloat16)


def solution(mesh):
    placed = (
        P(("sp", "tp"), None),
        P(),
        P(None, "tp"),
        P(None, "tp"),
        P(None, "tp"),
        P(None, "tp"),
        P(None, "tp"),
        P(None, "sp", "tp"),
        P(),
        P(None, "tp"),
        P(None, "tp"),
        P(None, "tp"),
        P("tp"),
        P(),
        P(),
        P(),
    )
    return jax.shard_map(
        on_device, mesh=mesh, in_specs=placed, out_specs=P(("sp", "tp"), None), check_vma=False
    )
```

profile of v0, /device:TPU:0, one launch (start us, length us, event | category | flops | bytes accessed | tf_op | source)
XLA Modules:
  0.0 309.0 jit_solution(12246848401442448760)
XLA Ops:
  6.5 1.4 fusion.22
  7.9 2.0 fusion.24
  12.5 2.4 constant_dynamic-update-slice_fusion.6
  21.5 14.0 %all-gather.2.cloned.1.call-done = bf16[512,2048]{1,0:T(8,128)(2,1)} async-done(((bf16[128,2048]{1,0:T(8,128)(2,1)}), bf16[512,2048]{1,0:T(8,128)(2,1)}) %all-gather.2.cloned.1.call-update) | async-done | bytes 2097168 | tf_op jit(solution)/shard_map/all_gather | solution.py:151
  35.4 7.7 %convolution_convert_fusion = bf16[512,1792]{1,0:T(8,128)(2,1)S(1)} fusion(bf16[512,2048]{1,0:T(8,128)(2,1)} %all-gather.2.cloned.1.call-done, bf16[2048,1792]{1,0:T(8,128)(2,1)} %constant_dynamic-update-slice_fusion), kind=kOutput, calls=%fused_computation.23 | convolution fusion | flops 3759013888 | bytes 11272192 | tf_op jit(solution)/shard_map/dot_general | solution.py:150
  44.5 1.4 fusion.37
  52.0 1.9 copy-done
  56.0 4.8 %rev.17 = f32[2,512,128]{2,1,0:T(8,128)} reverse(f32[2,512,128]{2,1,0:T(8,128)} %get-tuple-element.393), dimensions={1} | reverse | bytes 1048576 | tf_op jit(solution)/shard_map/jit(_flip)/rev | solution.py:173
  64.0 3.2 %exponential_multiply_fusion.3 = (f32[2,8,64,128]{3,1,2,0:T(8,128)S(1)}, f32[2,8,64,128]{3,1,2,0:T(8,128)}, f32[2,8,64,128]{3,1,2,0:T(8,128)}, f32[2,8,64,128]{3,1,2,0:T(8,128)}, f32[2,8,64,128]{3,1,2,0:T(8,128)}) fusion(f32[2,8,64,128]{3,1,2,0:T(8,128)} %copy-done.8, f32[2,8,64,128]{3,2,1,0:T(8,128)} %bitcast.229, f32[2,8,128]{2,1,0:T(8,128)S(1)} %get-tuple-element.376, ...), kind=kLoop, calls=%fused_computation.88 | loop fusion | flops 1048576 | bytes 4218880 | tf_op jit(solution)/shard_map/mul | solution.py:57
  67.2 2.8 convolution_bitcast_fusion
  71.1 19.3 %while.18 = (s32[]{:T(128)}, f32[2,128,128]{2,1,0:T(8,128)S(1)}, f32[8,2,128,128]{3,2,1,0:T(8,128)}, f32[8,2,128]{2,0,1:T(8,128)}, f32[8,2,128,128]{3,2,0,1:T(8,128)}, /*index=5*/s32[]{:T(128)}, s32[]{:T(128)}) while((s32[]{:T(128)}, f32[2,128,128]{2,1,0:T(8,128)S(1)}, f32[8,2,128,128]{3,2,1,0:T(8,128)}, ...), condition=%wide.region_11.12_spmd.clone, body=%wide.region_10.11_spmd.clone.sunk | while | flops 131075 | bytes 659040 | solution.py:68
  90.5 2.9 exponential_multiply_fusion.6
  93.4 2.0 convolution_bitcast_fusion.1
  95.5 14.2 %while.17 = (s32[]{:T(128)}, f32[2,128,128]{2,1,0:T(8,128)S(1)}, f32[8,2,128,128]{3,2,1,0:T(8,128)S(1)}, f32[8,2,128]{2,0,1:T(8,128)}, f32[8,2,128,128]{3,2,0,1:T(8,128)}, /*index=5*/s32[]{:T(128)}, s32[]{:T(128)}) while((s32[]{:T(128)}, f32[2,128,128]{2,1,0:T(8,128)S(1)}, f32[8,2,128,128]{3,2,1,0:T(8,128)S(1)}, ...), condition=%wide.region_3.4_spmd.clone, body=%wide.region_2.3_spmd.clone.sunk | while | flops 131075 | bytes 658532 | solution.py:68
  110.7 3.3 %fusion.18 = f32[2,2,512,128]{3,2,1,0:T(8,128)S(1)} fusion(f32[2,2,512,512]{2,3,1,0:T(8,128)} %copy-done, f32[2,2,512]{2,1,0:T(2,128)S(1)} %get-tuple-element.586, f32[2,2,512]{2,1,0:T(2,128)S(1)} %get-tuple-element.382, bf16[512,2,128,1]{2,1,0,3:T(2,128)(2,1)S(1)} %bitcast.231), kind=kOutput, calls=%fused_computation.30 | convolution fusion | flops 270794752 | bytes 5521408 | tf_op jit(solution)/shard_map/while/body/eval_jaxpr/hmqk,khv->hmqv/dot_general | solution.py:117
  114.0 144.8 %while.19 = (s32[]{:T(128)}, f32[2,2,512]{2,1,0:T(2,128)S(1)}, f32[2,2,512]{2,1,0:T(2,128)S(1)}, f32[2,2,512,128]{3,2,1,0:T(8,128)S(1)}, bf16[512,256]{0,1:T(8,1...) while((s32[]{:T(128)}, f32[2,2,512]{2,1,0:T(2,128)S(1)}, ...), condition=%wide.region_15.16_spmd.clone, body=%wide.region_12.15_spmd.clone.sunk | while | flops 408752128 | bytes 20326764 | solution.py:214
  114.3 1.5 collective-permute-start
  115.9 3.4 %collective-permute-start.2 = (bf16[2,128,128]{2,1,0:T(8,128)(2,1)S(1)}, bf16[2,128,128]{2,1,0:T(8,128)(2,1)S(1)}, u32[]{:S(2)}, u32[]{:S(2)}) collective-permute-start(bf16[2,128,128]{2,1,0:T(8,128)(2,1)S(1)} %fusion.100), channel_id=1, source_target_pairs={{0,4},{4,8},{8,12},{12,16},{16,20},{20,24},{24,28},{1,5},{5,9},{9,... | collective-permute-start | bytes 196616 | tf_op jit(solution)/shard_map/while/body/eval_jaxpr/ppermute | solution.py:28
  119.3 1.4 fusion.101
  122.0 2.7 collective-permute-start.1
  124.7 2.5 collective-permute-done.3
  129.4 3.9 %collective-permute-done.1 = bf16[512,256]{0,1:T(8,128)(2,1)S(1)} collective-permute-done((bf16[512,256]{0,1:T(8,128)(2,1)}, bf16[512,256]{0,1:T(8,128)(2,1)S(1)}, u32[]{:S(2)}, u32[]{:S(2)}) %collective-permute-start.1) | collective-permute-done | bytes 262176 | tf_op jit(solution)/shard_map/while/body/eval_jaxpr/ppermute | solution.py:22
  136.8 3.7 %collective-permute-start.2 = (bf16[2,128,128]{2,1,0:T(8,128)(2,1)S(1)}, bf16[2,128,128]{2,1,0:T(8,128)(2,1)S(1)}, u32[]{:S(2)}, u32[]{:S(2)}) collective-permute-start(bf16[2,128,128]{2,1,0:T(8,128)(2,1)S(1)} %fusion.100), channel_id=1, source_target_pairs={{0,4},{4,8},{8,12},{12,16},{16,20},{20,24},{24,28},{1,5},{5,9},{9,... | collective-permute-start | bytes 196616 | tf_op jit(solution)/shard_map/while/body/eval_jaxpr/ppermute | solution.py:28
  140.5 1.4 fusion.101
  143.2 2.7 collective-permute-start.1
  145.9 8.1 %collective-permute-done.3 = bf16[2,128,128]{2,1,0:T(8,128)(2,1)} collective-permute-done((bf16[2,128,128]{2,1,0:T(8,128)(2,1)}, bf16[2,128,128]{2,1,0:T(8,128)(2,1)}, u32[]{:S(2)}, u32[]{:S(2)}) %collective-permute-start.3) | collective-permute-done | bytes 65568 | tf_op jit(solution)/shard_map/while/body/eval_jaxpr/ppermute | solution.py:28
  156.2 1.3 fusion.99
  159.7 3.7 %collective-permute-start.2 = (bf16[2,128,128]{2,1,0:T(8,128)(2,1)S(1)}, bf16[2,128,128]{2,1,0:T(8,128)(2,1)S(1)}, u32[]{:S(2)}, u32[]{:S(2)}) collective-permute-start(bf16[2,128,128]{2,1,0:T(8,128)(2,1)S(1)} %fusion.100), channel_id=1, source_target_pairs={{0,4},{4,8},{8,12},{12,16},{16,20},{20,24},{24,28},{1,5},{5,9},{9,... | collective-permute-start | bytes 196616 | tf_op jit(solution)/shard_map/while/body/eval_jaxpr/ppermute | solution.py:28
  163.4 1.4 fusion.101
  166.1 2.7 collective-permute-start.1
  168.8 3.1 collective-permute-done.3
  174.1 2.1 collective-permute-done.1
  179.6 2.8 collective-permute-start.2
  182.5 1.4 fusion.101
  185.2 2.7 collective-permute-start.1
  187.9 4.7 %collective-permute-done.3 = bf16[2,128,128]{2,1,0:T(8,128)(2,1)} collective-permute-done((bf16[2,128,128]{2,1,0:T(8,128)(2,1)}, bf16[2,128,128]{2,1,0:T(8,128)(2,1)}, u32[]{:S(2)}, u32[]{:S(2)}) %collective-permute-start.3) | collective-permute-done | bytes 65568 | tf_op jit(solution)/shard_map/while/body/eval_jaxpr/ppermute | solution.py:28
  194.8 1.4 collective-permute-done.1
  199.6 2.0 collective-permute-start.2
  201.6 1.4 fusion.101
  204.3 2.7 collective-permute-start.1
  207.0 3.2 %collective-permute-done.3 = bf16[2,128,128]{2,1,0:T(8,128)(2,1)} collective-permute-done((bf16[2,128,128]{2,1,0:T(8,128)(2,1)}, bf16[2,128,128]{2,1,0:T(8,128)(2,1)}, u32[]{:S(2)}, u32[]{:S(2)}) %collective-permute-start.3) | collective-permute-done | bytes 65568 | tf_op jit(solution)/shard_map/while/body/eval_jaxpr/ppermute | solution.py:28
  212.5 3.7 %collective-permute-done.1 = bf16[512,256]{0,1:T(8,128)(2,1)S(1)} collective-permute-done((bf16[512,256]{0,1:T(8,128)(2,1)}, bf16[512,256]{0,1:T(8,128)(2,1)S(1)}, u32[]{:S(2)}, u32[]{:S(2)}) %collective-permute-start.1) | collective-permute-done | bytes 262176 | tf_op jit(solution)/shard_map/while/body/eval_jaxpr/ppermute | solution.py:22
  220.9 1.4 fusion.101
  223.5 2.7 collective-permute-start.1
  226.3 5.5 %collective-permute-done.3 = bf16[2,128,128]{2,1,0:T(8,128)(2,1)} collective-permute-done((bf16[2,128,128]{2,1,0:T(8,128)(2,1)}, bf16[2,128,128]{2,1,0:T(8,128)(2,1)}, u32[]{:S(2)}, u32[]{:S(2)}) %collective-permute-start.3) | collective-permute-done | bytes 65568 | tf_op jit(solution)/shard_map/while/body/eval_jaxpr/ppermute | solution.py:28
  234.1 2.1 collective-permute-done.1
  239.5 2.5 collective-permute-start.2
  242.0 1.4 fusion.101
  244.7 2.7 collective-permute-start.1
  247.4 4.4 %collective-permute-done.3 = bf16[2,128,128]{2,1,0:T(8,128)(2,1)} collective-permute-done((bf16[2,128,128]{2,1,0:T(8,128)(2,1)}, bf16[2,128,128]{2,1,0:T(8,128)(2,1)}, u32[]{:S(2)}, u32[]{:S(2)}) %collective-permute-start.3) | collective-permute-done | bytes 65568 | tf_op jit(solution)/shard_map/while/body/eval_jaxpr/ppermute | solution.py:28
  254.0 2.1 collective-permute-done.1
  262.1 1.8 convert_element_type.94
  263.9 4.0 %all-to-all-start.1 = ((bf16[4,128,256]{2,1,0:T(8,128)(2,1)}), bf16[4,128,256]{2,1,0:T(8,128)(2,1)}, u32[]{:S(2)}, u32[]{:S(2)}) async-start(bf16[4,128,256]{2,1,0:T(8,128)(2,1)} %convert_element_type.94), calls=%async_computation.1 | async-start | bytes 524288 | tf_op jit(solution)/shard_map/all_to_all | solution.py:229
  269.0 1.3 fusion.59
  270.4 3.0 convolution_add_fusion.2
  273.4 2.0 copy.73
  277.5 2.2 convolution_select_fusion
  280.4 2.1 convolution_add_fusion.1
  282.7 1.7 convolution_add_fusion.3
  285.2 1.7 multiply_reduce_fusion.1
  287.8 3.4 %all-to-all-start = ((bf16[4,128,256]{1,2,0:T(8,128)(2,1)}), bf16[4,128,256]{1,2,0:T(8,128)(2,1)S(1)}, u32[]{:S(2)}, u32[]{:S(2)}) async-start(bf16[4,128,256]{1,2,0:T(8,128)(2,1)} %copy.82), calls=%async_computation | async-start | bytes 524288 | tf_op jit(solution)/shard_map/all_to_all | solution.py:228
  292.4 4.8 %all-to-all-done = bf16[4,128,256]{1,2,0:T(8,128)(2,1)S(1)} async-done(((bf16[4,128,256]{1,2,0:T(8,128)(2,1)}), bf16[4,128,256]{1,2,0:T(8,128)(2,1)S(1)}, u32[]{:S(2)}, u32[]{:S(2)}) %all-to-all-start) | async-done | bytes 262176 | tf_op jit(solution)/shard_map/all_to_all | solution.py:228
  297.2 3.1 fusion.61
  300.7 1.5 fusion.14
  (301 shorter events, 115.0 us)
Async XLA Ops:
  6.5 8.3 %copy-start.14 = (bf16[2048,256]{1,0:T(8,128)(2,1)S(1)}, bf16[2048,256]{1,0:T(8,128)(2,1)}, u32[]{:S(2)}) copy-start(bf16[2048,256]{1,0:T(8,128)(2,1)} %param.25) | copy-start | bytes 3145732
  6.5 9.4 %copy-start.15 = (bf16[2048,256]{1,0:T(8,128)(2,1)S(1)}, bf16[2048,256]{1,0:T(8,128)(2,1)}, u32[]{:S(2)}) copy-start(bf16[2048,256]{1,0:T(8,128)(2,1)} %param.26) | copy-start | bytes 3145732
  6.5 28.9 %all-gather.2.cloned.1.call-start = ((), (), s32[]{:S(2)}) async-start(), calls=%async_computation.2 | async-start | bytes 2621440 | tf_op jit(solution)/shard_map/all_gather | solution.py:151
  10.0 7.0 %copy-start.16 = (bf16[2048,256]{1,0:T(8,128)(2,1)S(1)}, bf16[2048,256]{1,0:T(8,128)(2,1)}, u32[]{:S(2)}) copy-start(bf16[2048,256]{1,0:T(8,128)(2,1)} %param.27) | copy-start | bytes 3145732
  12.5 5.8 %copy-start.17 = (bf16[2048,256]{1,0:T(8,128)(2,1)S(1)}, bf16[2048,256]{1,0:T(8,128)(2,1)}, u32[]{:S(2)}) copy-start(bf16[2048,256]{1,0:T(8,128)(2,1)} %param.31) | copy-start | bytes 3145732
  14.9 4.5 %copy-start.18 = (bf16[2048,256]{1,0:T(8,128)(2,1)S(1)}, bf16[2048,256]{1,0:T(8,128)(2,1)}, u32[]{:S(2)}) copy-start(bf16[2048,256]{1,0:T(8,128)(2,1)} %param.32) | copy-start | bytes 3145732
  16.0 4.4 %copy-start.19 = (bf16[2048,256]{1,0:T(8,128)(2,1)S(1)}, bf16[2048,256]{1,0:T(8,128)(2,1)}, u32[]{:S(2)}) copy-start(bf16[2048,256]{1,0:T(8,128)(2,1)} %param.33) | copy-start | bytes 3145732
  46.5 5.4 %copy-start.8 = (f32[2,8,64,128]{3,1,2,0:T(8,128)}, f32[2,8,64,128]{3,1,2,0:T(8,128)S(1)}, u32[]{:S(2)}) copy-start(f32[2,8,64,128]{3,1,2,0:T(8,128)S(1)} %fusion.44) | copy-start | bytes 1572868
  47.5 4.4 %copy-start.1 = (f32[2,8,64,128]{3,1,2,0:T(8,128)}, f32[2,8,64,128]{3,1,2,0:T(8,128)S(1)}, u32[]{:S(2)}) copy-start(f32[2,8,64,128]{3,1,2,0:T(8,128)S(1)} %fusion.48) | copy-start | bytes 1572868
  51.9 1.9 copy-start
  51.9 2.8 copy-start.13
  51.9 2.5 slice-start
  51.9 2.6 copy-start.2
  53.9 2.1 slice-start.1
  53.9 2.1 copy-start.9
  90.5 5.0 %copy-start.7 = (bf16[2,512,128]{2,1,0:T(8,128)(2,1)}, bf16[2,512,128]{2,1,0:T(8,128)(2,1)S(1)}, u32[]{:S(2)}) copy-start(bf16[2,512,128]{2,1,0:T(8,128)(2,1)S(1)} %copy.51) | copy-start | bytes 786436
  90.5 20.2 %copy-start.20 = (bf16[512,2,128]{2,1,0:T(2,128)(2,1)S(1)}, bf16[512,2,128]{2,1,0:T(2,128)(2,1)}, u32[]{:S(2)}) copy-start(bf16[512,2,128]{2,1,0:T(2,128)(2,1)} %squeeze.48) | copy-start | bytes 786436
  109.7 1.0 copy-start.4
  114.2 1.5 copy-start.22
  114.3 13.8 %collective-permute-start = (bf16[512,256]{0,1:T(8,128)(2,1)}, bf16[512,256]{0,1:T(8,128)(2,1)S(1)}, u32[]{:S(2)}, u32[]{:S(2)}) collective-permute-start(bf16[512,256]{0,1:T(8,128)(2,1)} %get-tuple-element.604), channel_id=1, source_target_pairs={{0,4},{4,8},{8,12},{12,16},{16,20},{20,24},{24,28},{28,0},{1,5},{5... | collective-permute-start | bytes 786440 | tf_op jit(solution)/shard_map/while/body/eval_jaxpr/ppermute | solution.py:22
  115.9 8.8 %collective-permute-start.2 = (bf16[2,128,128]{2,1,0:T(8,128)(2,1)S(1)}, bf16[2,128,128]{2,1,0:T(8,128)(2,1)S(1)}, u32[]{:S(2)}, u32[]{:S(2)}) collective-permute-start(bf16[2,128,128]{2,1,0:T(8,128)(2,1)S(1)} %fusion.100), channel_id=1, source_target_pairs={{0,4},{4,8},{8,12},{12,16},{16,20},{20,24},{24,28},{1,5},{5,9},{9,... | collective-permute-start | bytes 196616 | tf_op jit(solution)/shard_map/while/body/eval_jaxpr/ppermute | solution.py:28
  120.7 6.5 %collective-permute-start.3 = (bf16[2,128,128]{2,1,0:T(8,128)(2,1)}, bf16[2,128,128]{2,1,0:T(8,128)(2,1)}, u32[]{:S(2)}, u32[]{:S(2)}) collective-permute-start(bf16[2,128,128]{2,1,0:T(8,128)(2,1)} %fusion.101), channel_id=1, source_target_pairs={{4,0},{8,4},{12,8},{16,12},{20,16},{24,20},{28,24},{5,1},{9,5},{13... | collective-permute-start | bytes 196616 | tf_op jit(solution)/shard_map/while/body/eval_jaxpr/ppermute | solution.py:28
  122.0 11.4 %collective-permute-start.1 = (bf16[512,256]{0,1:T(8,128)(2,1)}, bf16[512,256]{0,1:T(8,128)(2,1)S(1)}, u32[]{:S(2)}, u32[]{:S(2)}) collective-permute-start(bf16[512,256]{0,1:T(8,128)(2,1)} %get-tuple-element.605), channel_id=1, source_target_pairs={{0,4},{4,8},{8,12},{12,16},{16,20},{20,24},{24,28},{28,0},{1,5},{5... | collective-permute-start | bytes 786440 | tf_op jit(solution)/shard_map/while/body/eval_jaxpr/ppermute | solution.py:22
  129.4 6.7 %copy-start.23 = (f32[2,128]{1,0:T(2,128)S(1)}, f32[2,128]{1,0:T(2,128)}, u32[]{:S(2)}) copy-start(f32[2,128]{1,0:T(2,128)} %copy-done.22) | copy-start | bytes 3076 | tf_op jit(solution)/shard_map/while
  136.1 18.7 %collective-permute-start = (bf16[512,256]{0,1:T(8,128)(2,1)}, bf16[512,256]{0,1:T(8,128)(2,1)S(1)}, u32[]{:S(2)}, u32[]{:S(2)}) collective-permute-start(bf16[512,256]{0,1:T(8,128)(2,1)} %get-tuple-element.604), channel_id=1, source_target_pairs={{0,4},{4,8},{8,12},{12,16},{16,20},{20,24},{24,28},{28,0},{1,5},{5... | collective-permute-start | bytes 786440 | tf_op jit(solution)/shard_map/while/body/eval_jaxpr/ppermute | solution.py:22
  136.8 9.1 %collective-permute-start.2 = (bf16[2,128,128]{2,1,0:T(8,128)(2,1)S(1)}, bf16[2,128,128]{2,1,0:T(8,128)(2,1)S(1)}, u32[]{:S(2)}, u32[]{:S(2)}) collective-permute-start(bf16[2,128,128]{2,1,0:T(8,128)(2,1)S(1)} %fusion.100), channel_id=1, source_target_pairs={{0,4},{4,8},{8,12},{12,16},{16,20},{20,24},{24,28},{1,5},{5,9},{9,... | collective-permute-start | bytes 196616 | tf_op jit(solution)/shard_map/while/body/eval_jaxpr/ppermute | solution.py:28
  141.9 12.1 %collective-permute-start.3 = (bf16[2,128,128]{2,1,0:T(8,128)(2,1)}, bf16[2,128,128]{2,1,0:T(8,128)(2,1)}, u32[]{:S(2)}, u32[]{:S(2)}) collective-permute-start(bf16[2,128,128]{2,1,0:T(8,128)(2,1)} %fusion.101), channel_id=1, source_target_pairs={{4,0},{8,4},{12,8},{16,12},{20,16},{24,20},{28,24},{5,1},{9,5},{13... | collective-permute-start | bytes 196616 | tf_op jit(solution)/shard_map/while/body/eval_jaxpr/ppermute | solution.py:28
  143.2 13.1 %collective-permute-start.1 = (bf16[512,256]{0,1:T(8,128)(2,1)}, bf16[512,256]{0,1:T(8,128)(2,1)S(1)}, u32[]{:S(2)}, u32[]{:S(2)}) collective-permute-start(bf16[512,256]{0,1:T(8,128)(2,1)} %get-tuple-element.605), channel_id=1, source_target_pairs={{0,4},{4,8},{8,12},{12,16},{16,20},{20,24},{24,28},{28,0},{1,5},{5... | collective-permute-start | bytes 786440 | tf_op jit(solution)/shard_map/while/body/eval_jaxpr/ppermute | solution.py:22
  156.2 2.8 copy-start.23
  159.0 13.8 %collective-permute-start = (bf16[512,256]{0,1:T(8,128)(2,1)}, bf16[512,256]{0,1:T(8,128)(2,1)S(1)}, u32[]{:S(2)}, u32[]{:S(2)}) collective-permute-start(bf16[512,256]{0,1:T(8,128)(2,1)} %get-tuple-element.604), channel_id=1, source_target_pairs={{0,4},{4,8},{8,12},{12,16},{16,20},{20,24},{24,28},{28,0},{1,5},{5... | collective-permute-start | bytes 786440 | tf_op jit(solution)/shard_map/while/body/eval_jaxpr/ppermute | solution.py:22
  159.7 9.1 %collective-permute-start.2 = (bf16[2,128,128]{2,1,0:T(8,128)(2,1)S(1)}, bf16[2,128,128]{2,1,0:T(8,128)(2,1)S(1)}, u32[]{:S(2)}, u32[]{:S(2)}) collective-permute-start(bf16[2,128,128]{2,1,0:T(8,128)(2,1)S(1)} %fusion.100), channel_id=1, source_target_pairs={{0,4},{4,8},{8,12},{12,16},{16,20},{20,24},{24,28},{1,5},{5,9},{9,... | collective-permute-start | bytes 196616 | tf_op jit(solution)/shard_map/while/body/eval_jaxpr/ppermute | solution.py:28
  164.8 7.1 %collective-permute-start.3 = (bf16[2,128,128]{2,1,0:T(8,128)(2,1)}, bf16[2,128,128]{2,1,0:T(8,128)(2,1)}, u32[]{:S(2)}, u32[]{:S(2)}) collective-permute-start(bf16[2,128,128]{2,1,0:T(8,128)(2,1)} %fusion.101), channel_id=1, source_target_pairs={{4,0},{8,4},{12,8},{16,12},{20,16},{24,20},{28,24},{5,1},{9,5},{13... | collective-permute-start | bytes 196616 | tf_op jit(solution)/shard_map/while/body/eval_jaxpr/ppermute | solution.py:28
  166.1 10.1 %collective-permute-start.1 = (bf16[512,256]{0,1:T(8,128)(2,1)}, bf16[512,256]{0,1:T(8,128)(2,1)S(1)}, u32[]{:S(2)}, u32[]{:S(2)}) collective-permute-start(bf16[512,256]{0,1:T(8,128)(2,1)} %get-tuple-element.605), channel_id=1, source_target_pairs={{0,4},{4,8},{8,12},{12,16},{16,20},{20,24},{24,28},{28,0},{1,5},{5... | collective-permute-start | bytes 786440 | tf_op jit(solution)/shard_map/while/body/eval_jaxpr/ppermute | solution.py:22
  174.1 4.8 %copy-start.23 = (f32[2,128]{1,0:T(2,128)S(1)}, f32[2,128]{1,0:T(2,128)}, u32[]{:S(2)}) copy-start(f32[2,128]{1,0:T(2,128)} %copy-done.22) | copy-start | bytes 3076 | tf_op jit(solution)/shard_map/while
  178.9 14.5 %collective-permute-start = (bf16[512,256]{0,1:T(8,128)(2,1)}, bf16[512,256]{0,1:T(8,128)(2,1)S(1)}, u32[]{:S(2)}, u32[]{:S(2)}) collective-permute-start(bf16[512,256]{0,1:T(8,128)(2,1)} %get-tuple-element.604), channel_id=1, source_target_pairs={{0,4},{4,8},{8,12},{12,16},{16,20},{20,24},{24,28},{28,0},{1,5},{5... | collective-permute-start | bytes 786440 | tf_op jit(solution)/shard_map/while/body/eval_jaxpr/ppermute | solution.py:22
  179.6 8.2 %collective-permute-start.2 = (bf16[2,128,128]{2,1,0:T(8,128)(2,1)S(1)}, bf16[2,128,128]{2,1,0:T(8,128)(2,1)S(1)}, u32[]{:S(2)}, u32[]{:S(2)}) collective-permute-start(bf16[2,128,128]{2,1,0:T(8,128)(2,1)S(1)} %fusion.100), channel_id=1, source_target_pairs={{0,4},{4,8},{8,12},{12,16},{16,20},{20,24},{24,28},{1,5},{5,9},{9,... | collective-permute-start | bytes 196616 | tf_op jit(solution)/shard_map/while/body/eval_jaxpr/ppermute | solution.py:28
  183.9 8.7 %collective-permute-start.3 = (bf16[2,128,128]{2,1,0:T(8,128)(2,1)}, bf16[2,128,128]{2,1,0:T(8,128)(2,1)}, u32[]{:S(2)}, u32[]{:S(2)}) collective-permute-start(bf16[2,128,128]{2,1,0:T(8,128)(2,1)} %fusion.101), channel_id=1, source_target_pairs={{4,0},{8,4},{12,8},{16,12},{20,16},{24,20},{28,24},{5,1},{9,5},{13... | collective-permute-start | bytes 196616 | tf_op jit(solution)/shard_map/while/body/eval_jaxpr/ppermute | solution.py:28
  185.2 11.0 %collective-permute-start.1 = (bf16[512,256]{0,1:T(8,128)(2,1)}, bf16[512,256]{0,1:T(8,128)(2,1)S(1)}, u32[]{:S(2)}, u32[]{:S(2)}) collective-permute-start(bf16[512,256]{0,1:T(8,128)(2,1)} %get-tuple-element.605), channel_id=1, source_target_pairs={{0,4},{4,8},{8,12},{12,16},{16,20},{20,24},{24,28},{28,0},{1,5},{5... | collective-permute-start | bytes 786440 | tf_op jit(solution)/shard_map/while/body/eval_jaxpr/ppermute | solution.py:22
  194.8 4.1 %copy-start.23 = (f32[2,128]{1,0:T(2,128)S(1)}, f32[2,128]{1,0:T(2,128)}, u32[]{:S(2)}) copy-start(f32[2,128]{1,0:T(2,128)} %copy-done.22) | copy-start | bytes 3076 | tf_op jit(solution)/shard_map/while
  198.9 12.1 %collective-permute-start = (bf16[512,256]{0,1:T(8,128)(2,1)}, bf16[512,256]{0,1:T(8,128)(2,1)S(1)}, u32[]{:S(2)}, u32[]{:S(2)}) collective-permute-start(bf16[512,256]{0,1:T(8,128)(2,1)} %get-tuple-element.604), channel_id=1, source_target_pairs={{0,4},{4,8},{8,12},{12,16},{16,20},{20,24},{24,28},{28,0},{1,5},{5... | collective-permute-start | bytes 786440 | tf_op jit(solution)/shard_map/while/body/eval_jaxpr/ppermute | solution.py:22
  199.6 7.4 %collective-permute-start.2 = (bf16[2,128,128]{2,1,0:T(8,128)(2,1)S(1)}, bf16[2,128,128]{2,1,0:T(8,128)(2,1)S(1)}, u32[]{:S(2)}, u32[]{:S(2)}) collective-permute-start(bf16[2,128,128]{2,1,0:T(8,128)(2,1)S(1)} %fusion.100), channel_id=1, source_target_pairs={{0,4},{4,8},{8,12},{12,16},{16,20},{20,24},{24,28},{1,5},{5,9},{9,... | collective-permute-start | bytes 196616 | tf_op jit(solution)/shard_map/while/body/eval_jaxpr/ppermute | solution.py:28
  203.0 7.2 %collective-permute-start.3 = (bf16[2,128,128]{2,1,0:T(8,128)(2,1)}, bf16[2,128,128]{2,1,0:T(8,128)(2,1)}, u32[]{:S(2)}, u32[]{:S(2)}) collective-permute-start(bf16[2,128,128]{2,1,0:T(8,128)(2,1)} %fusion.101), channel_id=1, source_target_pairs={{4,0},{8,4},{12,8},{16,12},{20,16},{24,20},{28,24},{5,1},{9,5},{13... | collective-permute-start | bytes 196616 | tf_op jit(solution)/shard_map/while/body/eval_jaxpr/ppermute | solution.py:28
  204.3 11.9 %collective-permute-start.1 = (bf16[512,256]{0,1:T(8,128)(2,1)}, bf16[512,256]{0,1:T(8,128)(2,1)S(1)}, u32[]{:S(2)}, u32[]{:S(2)}) collective-permute-start(bf16[512,256]{0,1:T(8,128)(2,1)} %get-tuple-element.605), channel_id=1, source_target_pairs={{0,4},{4,8},{8,12},{12,16},{16,20},{20,24},{24,28},{28,0},{1,5},{5... | collective-permute-start | bytes 786440 | tf_op jit(solution)/shard_map/while/body/eval_jaxpr/ppermute | solution.py:22
  212.4 6.5 %copy-start.23 = (f32[2,128]{1,0:T(2,128)S(1)}, f32[2,128]{1,0:T(2,128)}, u32[]{:S(2)}) copy-start(f32[2,128]{1,0:T(2,128)} %copy-done.22) | copy-start | bytes 3076 | tf_op jit(solution)/shard_map/while
  218.9 13.8 %collective-permute-start = (bf16[512,256]{0,1:T(8,128)(2,1)}, bf16[512,256]{0,1:T(8,128)(2,1)S(1)}, u32[]{:S(2)}, u32[]{:S(2)}) collective-permute-start(bf16[512,256]{0,1:T(8,128)(2,1)} %get-tuple-element.604), channel_id=1, source_target_pairs={{0,4},{4,8},{8,12},{12,16},{16,20},{20,24},{24,28},{28,0},{1,5},{5... | collective-permute-start | bytes 786440 | tf_op jit(solution)/shard_map/while/body/eval_jaxpr/ppermute | solution.py:22
  219.6 6.7 %collective-permute-start.2 = (bf16[2,128,128]{2,1,0:T(8,128)(2,1)S(1)}, bf16[2,128,128]{2,1,0:T(8,128)(2,1)S(1)}, u32[]{:S(2)}, u32[]{:S(2)}) collective-permute-start(bf16[2,128,128]{2,1,0:T(8,128)(2,1)S(1)} %fusion.100), channel_id=1, source_target_pairs={{0,4},{4,8},{8,12},{12,16},{16,20},{20,24},{24,28},{1,5},{5,9},{9,... | collective-permute-start | bytes 196616 | tf_op jit(solution)/shard_map/while/body/eval_jaxpr/ppermute | solution.py:28
  222.3 9.5 %collective-permute-start.3 = (bf16[2,128,128]{2,1,0:T(8,128)(2,1)}, bf16[2,128,128]{2,1,0:T(8,128)(2,1)}, u32[]{:S(2)}, u32[]{:S(2)}) collective-permute-start(bf16[2,128,128]{2,1,0:T(8,128)(2,1)} %fusion.101), channel_id=1, source_target_pairs={{4,0},{8,4},{12,8},{16,12},{20,16},{24,20},{28,24},{5,1},{9,5},{13... | collective-permute-start | bytes 196616 | tf_op jit(solution)/shard_map/while/body/eval_jaxpr/ppermute | solution.py:28
  223.5 12.6 %collective-permute-start.1 = (bf16[512,256]{0,1:T(8,128)(2,1)}, bf16[512,256]{0,1:T(8,128)(2,1)S(1)}, u32[]{:S(2)}, u32[]{:S(2)}) collective-permute-start(bf16[512,256]{0,1:T(8,128)(2,1)} %get-tuple-element.605), channel_id=1, source_target_pairs={{0,4},{4,8},{8,12},{12,16},{16,20},{20,24},{24,28},{28,0},{1,5},{5... | collective-permute-start | bytes 786440 | tf_op jit(solution)/shard_map/while/body/eval_jaxpr/ppermute | solution.py:22
  234.0 4.8 %copy-start.23 = (f32[2,128]{1,0:T(2,128)S(1)}, f32[2,128]{1,0:T(2,128)}, u32[]{:S(2)}) copy-start(f32[2,128]{1,0:T(2,128)} %copy-done.22) | copy-start | bytes 3076 | tf_op jit(solution)/shard_map/while
  238.9 13.8 %collective-permute-start = (bf16[512,256]{0,1:T(8,128)(2,1)}, bf16[512,256]{0,1:T(8,128)(2,1)S(1)}, u32[]{:S(2)}, u32[]{:S(2)}) collective-permute-start(bf16[512,256]{0,1:T(8,128)(2,1)} %get-tuple-element.604), channel_id=1, source_target_pairs={{0,4},{4,8},{8,12},{12,16},{16,20},{20,24},{24,28},{28,0},{1,5},{5... | collective-permute-start | bytes 786440 | tf_op jit(solution)/shard_map/while/body/eval_jaxpr/ppermute | solution.py:22
  239.5 7.8 %collective-permute-start.2 = (bf16[2,128,128]{2,1,0:T(8,128)(2,1)S(1)}, bf16[2,128,128]{2,1,0:T(8,128)(2,1)S(1)}, u32[]{:S(2)}, u32[]{:S(2)}) collective-permute-start(bf16[2,128,128]{2,1,0:T(8,128)(2,1)S(1)} %fusion.100), channel_id=1, source_target_pairs={{0,4},{4,8},{8,12},{12,16},{16,20},{20,24},{24,28},{1,5},{5,9},{9,... | collective-permute-start | bytes 196616 | tf_op jit(solution)/shard_map/while/body/eval_jaxpr/ppermute | solution.py:28
  243.4 8.4 %collective-permute-start.3 = (bf16[2,128,128]{2,1,0:T(8,128)(2,1)}, bf16[2,128,128]{2,1,0:T(8,128)(2,1)}, u32[]{:S(2)}, u32[]{:S(2)}) collective-permute-start(bf16[2,128,128]{2,1,0:T(8,128)(2,1)} %fusion.101), channel_id=1, source_target_pairs={{4,0},{8,4},{12,8},{16,12},{20,16},{24,20},{28,24},{5,1},{9,5},{13... | collective-permute-start | bytes 196616 | tf_op jit(solution)/shard_map/while/body/eval_jaxpr/ppermute | solution.py:28
  244.7 11.4 %collective-permute-start.1 = (bf16[512,256]{0,1:T(8,128)(2,1)}, bf16[512,256]{0,1:T(8,128)(2,1)S(1)}, u32[]{:S(2)}, u32[]{:S(2)}) collective-permute-start(bf16[512,256]{0,1:T(8,128)(2,1)} %get-tuple-element.605), channel_id=1, source_target_pairs={{0,4},{4,8},{8,12},{12,16},{16,20},{20,24},{24,28},{28,0},{1,5},{5... | collective-permute-start | bytes 786440 | tf_op jit(solution)/shard_map/while/body/eval_jaxpr/ppermute | solution.py:22
  254.0 4.8 %copy-start.23 = (f32[2,128]{1,0:T(2,128)S(1)}, f32[2,128]{1,0:T(2,128)}, u32[]{:S(2)}) copy-start(f32[2,128]{1,0:T(2,128)} %copy-done.22) | copy-start | bytes 3076 | tf_op jit(solution)/shard_map/while
  258.8 9.1 %copy-start.21 = (pred[64,64]{1,0:T(8,128)(4,1)S(1)}, pred[64,64]{1,0:T(8,128)(4,1)}, u32[]{:S(2)}) copy-start(pred[64,64]{1,0:T(8,128)(4,1)} %iota_compare_fusion) | copy-start | bytes 12292
  258.8 11.6 %copy-start.5 = (f32[8,2,128,128]{3,2,1,0:T(8,128)S(1)}, f32[8,2,128,128]{3,2,1,0:T(8,128)}, u32[]{:S(2)}) copy-start(f32[8,2,128,128]{3,2,1,0:T(8,128)} %copy-done.4) | copy-start | bytes 3145732
  259.2 8.8 %copy-start.10 = (f32[2,8,64,128]{3,1,2,0:T(8,128)S(1)}, f32[2,8,64,128]{3,1,2,0:T(8,128)}, u32[]{:S(2)}) copy-start(f32[2,8,64,128]{3,1,2,0:T(8,128)} %get-tuple-element.355) | copy-start | bytes 1572868
  259.2 8.8 %copy-start.11 = (f32[2,8,64,128]{3,1,2,0:T(8,128)S(1)}, f32[2,8,64,128]{3,1,2,0:T(8,128)}, u32[]{:S(2)}) copy-start(f32[2,8,64,128]{3,1,2,0:T(8,128)} %get-tuple-element.367) | copy-start | bytes 1572868
  263.9 23.9 %all-to-all-start.1 = ((bf16[4,128,256]{2,1,0:T(8,128)(2,1)}), bf16[4,128,256]{2,1,0:T(8,128)(2,1)}, u32[]{:S(2)}, u32[]{:S(2)}) async-start(bf16[4,128,256]{2,1,0:T(8,128)(2,1)} %convert_element_type.94), calls=%async_computation.1 | async-start | bytes 524288 | tf_op jit(solution)/shard_map/all_to_all | solution.py:229
  270.4 10.0 %copy-start.6 = (f32[8,2,128,128]{3,2,1,0:T(8,128)S(1)}, f32[8,2,128,128]{3,2,1,0:T(8,128)}, u32[]{:S(2)}) copy-start(f32[8,2,128,128]{3,2,1,0:T(8,128)} %get-tuple-element.177) | copy-start | bytes 3145732
  279.7 5.5 %copy-start.12 = (f32[2,512,128]{1,2,0:T(8,128)S(1)}, f32[2,512,128]{1,2,0:T(8,128)}, u32[]{:S(2)}) copy-start(f32[2,512,128]{1,2,0:T(8,128)} %copy.73) | copy-start | bytes 1572868
  280.4 6.5 %copy-start.24 = (f32[128]{0:T(128)S(1)}, f32[128]{0:T(128)}, u32[]{:S(2)}) copy-start(f32[128]{0:T(128)} %param.30) | copy-start | bytes 1540
  287.8 9.4 %all-to-all-start = ((bf16[4,128,256]{1,2,0:T(8,128)(2,1)}), bf16[4,128,256]{1,2,0:T(8,128)(2,1)S(1)}, u32[]{:S(2)}, u32[]{:S(2)}) async-start(bf16[4,128,256]{1,2,0:T(8,128)(2,1)} %copy.82), calls=%async_computation | async-start | bytes 524288 | tf_op jit(solution)/shard_map/all_to_all | solution.py:228
  297.2 3.4 %copy-start.3 = (bf16[1024,2048]{1,0:T(8,128)(2,1)S(1)}, bf16[1024,2048]{1,0:T(8,128)(2,1)}, u32[]{:S(2)}) copy-start(bf16[1024,2048]{1,0:T(8,128)(2,1)} %param.37) | copy-start | bytes 12582916
  (6 other events, 3.5 us)
Sparse Core Ops, SparseCore 0:
  10.1 25.2 all-gather.1
where the time goes:
time: 312 us; the launch traced here: 309 us
  waiting for transfers between devices  65.5 us (21%)
  other arithmetic  62.4 us (20%)
  local copies, waits for them, and re-layouts  59.9 us (19%)
  starting transfers between devices  56.8 us (18%)
  matrix products  49.2 us (16%)
  between operations  14 us (4%)
    ppermute x14, waiting for transfers between devices, passed_along_2(): return lax.ppermute(block, axis, route)  31.4 us
    ppermute x14, starting transfers between devices, passed_along_2(): return lax.ppermute(block, axis, route)  28.4 us
    ppermute x14, starting transfers between devices, passed_along(): lax.ppermute(value, axis, [(i, (i + by) % size) for i in range(size)])  20.9 us
    add x16, other arithmetic, advance(): return (factor[..., None] * running + added_state, running)  16.3 us
    ppermute x14, waiting for transfers between devices, passed_along(): lax.ppermute(value, axis, [(i, (i + by) % size) for i in range(size)])  15.3 us
    all_gather x1, waiting for transfers between devices, on_device(): lax.all_gather(normed, 'tp', axis=0, tiled=True)  14 us
    while x49, local copies, waits for them, and re-layouts  13 us
    dot_general x8, matrix products, absorb(): jnp.einsum('hmqk,khv->hmqv', weights_raw.astype(jnp.bfloat16), value_bloc...  12.2 us
  transfers between devices with their start and end apart: 31, of which 15 were waited for; matrix products, arithmetic and copies ran while one was open for 19% of the time, Pallas kernels for 0%

commit v1 on v0

v1 whole, which is shorter than its diff:
```python
import functools

import jax
import jax.numpy as jnp
from jax import lax
from jax.experimental import pallas as pl
from jax.experimental.pallas import tpu as pltpu
from jax.sharding import PartitionSpec as P

HK = 128
AK = 64
BLOCK = 64
LANES = 128
EPS = 1e-06
THETA = 500000.0
HIGHEST = lax.Precision.HIGHEST
F32 = jnp.float32
BF16 = jnp.bfloat16
PAD = 16


def rms_scale(values, gain):
    return values * lax.rsqrt(jnp.mean(values * values, axis=-1, keepdims=True) + EPS) * gain


def dot_t(a, b):
    return lax.dot_general(a, b, (((1,), (1,)), ((), ())), preferred_element_type=F32)


def dot_0(a, b):
    return lax.dot_general(a, b, (((0,), (0,)), ((), ())), preferred_element_type=F32)


def mixer_kernel(
    ranks, groups, heads, tile,
    proj, cosine, sine, leak, decay, lam, rec_gain, att_gain,
    out,
    kv, rest, swap, back, state_out, state_in, cums, adds, states, rec_sum, peak, total, mixed,
    kv_send, kv_recv, swap_send, rest_recv, state_send, state_recv, back_send, back_recv,
):
    me = lax.axis_index("sp")
    slot = lax.rem(me, groups)
    mine = lax.div(me, groups)
    length = proj.shape[1]
    rows = groups * length
    width = heads * LANES
    block_count = rows // BLOCK
    partner_slot = groups - 1 - slot
    partner = mine * groups + partner_slot
    blocks = ranks // groups
    own_rows = pl.ds(pl.multiple_of(slot * length, length), length)
    other_rows = pl.ds(pl.multiple_of(partner_slot * length, length), length)

    barrier = pltpu.get_barrier_semaphore()
    peers = []
    for k in range(1, blocks):
        peers.append(lax.rem(mine + k, blocks))
    for peer in peers:
        pl.semaphore_signal(barrier, inc=1, device_id={"sp": peer * groups + slot})
    if groups > 1:
        pl.semaphore_signal(barrier, inc=1, device_id={"sp": partner})

    lane = lax.broadcasted_iota(jnp.int32, (length, LANES), 1)
    low_half = lax.rem(lane, AK) < AK // 2

    def rotated(raw):
        wide = raw.astype(F32)
        turned = jnp.where(low_half, -pltpu.roll(wide, LANES - AK // 2, 1), pltpu.roll(wide, AK // 2, 1))
        return wide * cosine[...] + turned * sine[...]

    def prepare(head_group, key_value, others):
        for h in range(heads):
            at = h * LANES
            key_value[:, at : at + LANES] = rotated(proj[head_group, :, at : at + LANES]).astype(BF16)
        key_value[:, width : 2 * width] = proj[head_group, :, width : 2 * width]
        for h in range(heads):
            at = 2 * width + h * LANES
            others[:, h * LANES : (h + 1) * LANES] = (
                rotated(proj[head_group, :, at : at + LANES]) * AK ** (-0.5)
            ).astype(BF16)
        others[:, width:] = proj[head_group, :, 3 * width :]

    if groups > 1:
        prepare(partner_slot, swap.at[:, : 2 * width], swap.at[:, 2 * width :])
    prepare(slot, kv.at[mine, own_rows], rest.at[own_rows])
    pl.semaphore_wait(barrier, blocks - 1 + (groups - 1))

    def block_copy(source_rows, source_slot, peer):
        return pltpu.make_async_remote_copy(
            src_ref=kv.at[mine, source_rows],
            dst_ref=kv.at[mine, source_rows],
            send_sem=kv_send.at[peer, source_slot],
            recv_sem=kv_recv.at[mine, source_slot],
            device_id={"sp": peer * groups + slot},
        )

    def arrival(block, piece):
        piece_rows = pl.ds(pl.multiple_of(piece * length, length), length)
        return pltpu.make_async_remote_copy(
            src_ref=kv.at[block, piece_rows],
            dst_ref=kv.at[block, piece_rows],
            send_sem=kv_send.at[block, piece],
            recv_sem=kv_recv.at[block, piece],
            device_id={"sp": block * groups + slot},
        )

    if groups > 1:
        swap_kv = pltpu.make_async_remote_copy(
            src_ref=swap.at[:, : 2 * width],
            dst_ref=kv.at[mine, own_rows],
            send_sem=swap_send.at[0],
            recv_sem=kv_recv.at[mine, slot],
            device_id={"sp": partner},
        )
        swap_kv.start()
        swap_rest = pltpu.make_async_remote_copy(
            src_ref=swap.at[:, 2 * width :],
            dst_ref=rest.at[own_rows],
            send_sem=swap_send.at[1],
            recv_sem=rest_recv,
            device_id={"sp": partner},
        )
    own_copies = [block_copy(own_rows, slot, peer) for peer in peers]
    for copy in own_copies:
        copy.start()
    other_copies = []
    if groups > 1:
        swap_rest.start()
        arrival(mine, partner_slot).wait_recv()
        other_copies = [block_copy(other_rows, partner_slot, peer) for peer in peers]
        for copy in other_copies:
            copy.start()
        swap_rest.wait_recv()

    row_at = lax.broadcasted_iota(jnp.int32, (BLOCK, BLOCK), 0)
    col_at = lax.broadcasted_iota(jnp.int32, (BLOCK, BLOCK), 1)
    earlier = (row_at >= col_at, row_at <= col_at)
    triangles = tuple(mask.astype(F32) for mask in earlier)
    ends = (BLOCK - 1, 0)
    middles = (BLOCK // 2 - 1, BLOCK // 2)

    def rows_of(direction, step):
        index = step if direction == 0 else block_count - 1 - step
        return index, pl.ds(pl.multiple_of(index * BLOCK, BLOCK), BLOCK)

    def part(at, index, h):
        return rest[at, (index * heads + h) * LANES : (index * heads + h + 1) * LANES].astype(F32)

    def keys_of(at, direction, h):
        return leak[h, direction : direction + 1, :] * jax.nn.sigmoid(-part(at, 2 + direction, h))

    states[...] = jnp.zeros_like(states)
    rec_sum[...] = jnp.zeros_like(rec_sum)

    def first_pass(step, totals):
        after = []
        for h in range(heads):
            for d in range(2):
                index, at = rows_of(d, step)
                keys = keys_of(at, d, h)
                column = d * heads + h
                logs = jnp.log1p(-keys) + decay[at, column : column + 1]
                cum = jnp.dot(triangles[d], logs, precision=HIGHEST, preferred_element_type=F32)
                cums[h, d, at, :] = cum
                last = cum[ends[d] : ends[d] + 1, :]
                scaled = (keys * jnp.exp(last - cum)).astype(BF16)
                added = dot_0(part(at, 4, h).astype(BF16), scaled)
                adds[h, d, index] = added
                states[h, d] = states[h, d] * jnp.exp(last) + added
                after.append(totals[h * 2 + d] + last)
        return tuple(after)

    nothing = tuple(jnp.zeros((1, LANES), F32) for _ in range(2 * heads))
    sums = lax.fori_loop(0, block_count, first_pass, nothing, unroll=2)
    for h in range(heads):
        for d in range(2):
            state_out[d, h, :LANES, :] = states[h, d].astype(BF16)
            factor = jnp.broadcast_to(jnp.exp(sums[h * 2 + d]), (PAD, LANES))
            coarse = factor.astype(BF16)
            fine = (factor - coarse.astype(F32)).astype(BF16)
            first_row = lax.broadcasted_iota(jnp.int32, (PAD, LANES), 0) == 0
            state_out[d, h, LANES:, :] = jnp.where(first_row, coarse.astype(F32), fine.astype(F32)).astype(BF16)
    state_copies = []
    for peer in peers:
        copy = pltpu.make_async_remote_copy(
            src_ref=state_out.at[jnp.where(peer > mine, 0, 1)],
            dst_ref=state_in.at[mine],
            send_sem=state_send.at[peer],
            recv_sem=state_recv.at[mine],
            device_id={"sp": peer * groups + slot},
        )
        copy.start()
        state_copies.append(copy)

    lane_q = lax.broadcasted_iota(jnp.int32, (tile, LANES), 1)
    tiles = rows // tile
    peak[...] = jnp.full_like(peak, -jnp.inf)
    total[...] = jnp.zeros_like(total)
    mixed[...] = jnp.zeros_like(mixed)

    def attend(block):
        for h in range(heads):
            at = h * LANES

            def one_tile(index, carry):
                q_rows = pl.ds(pl.multiple_of(index * tile, tile), tile)
                queries = rest[q_rows, at : at + LANES]
                zero = jnp.zeros_like(queries)
                both = jnp.concatenate(
                    [jnp.where(lane_q < AK, queries, zero), jnp.where(lane_q < AK, zero, queries)], axis=0
                )
                scores = dot_t(both, kv[block, :, at : at + LANES])
                before = peak[h, index][:, :1]
                raised = jnp.maximum(before, jnp.max(scores, axis=-1, keepdims=True))
                shrink = jnp.exp(before - raised)
                expo = jnp.exp(scores - raised)
                sums_now = total[h, index][:, :1] * shrink + jnp.sum(expo, axis=-1, keepdims=True)
                product = jnp.dot(
                    expo.astype(BF16), kv[block, :, width + at : width + at + LANES], preferred_element_type=F32
                )
                mixed[h, index] = mixed[h, index] * shrink + product
                peak[h, index] = jnp.broadcast_to(raised, (2 * tile, LANES))
                total[h, index] = jnp.broadcast_to(sums_now, (2 * tile, LANES))
                return carry

            lax.fori_loop(0, tiles, one_tile, 0)

    attend(mine)

    def state_arrival(block):
        return pltpu.make_async_remote_copy(
            src_ref=state_out.at[0],
            dst_ref=state_in.at[block],
            send_sem=state_send.at[block],
            recv_sem=state_recv.at[block],
            device_id={"sp": block * groups + slot},
        )

    states[...] = jnp.zeros_like(states)

    def compose(d):
        def body(step, carry):
            block = step if d == 0 else blocks - 1 - step
            state_arrival(block).wait_recv()
            for h in range(heads):
                rows_last = state_in[block, h, LANES:, :].astype(F32)
                factor = rows_last[0:1] + rows_last[1:2]
                states[h, d] = states[h, d] * factor + state_in[block, h, :LANES, :].astype(F32)
            return carry

        return body

    lax.fori_loop(0, mine, compose(0), 0)
    lax.fori_loop(0, blocks - 1 - mine, compose(1), 0)

    def second_pass(step, carry):
        for h in range(heads):
            for d in range(2):
                index, at = rows_of(d, step)
                queries = jax.nn.silu(part(at, 1, h))
                keys = keys_of(at, d, h)
                cum = cums[h, d, at, :]
                middle = cum[middles[d] : middles[d] + 1, :]
                last = cum[ends[d] : ends[d] + 1, :]
                scores = dot_t(
                    (queries * jnp.exp(cum - middle)).astype(BF16), (keys * jnp.exp(middle - cum)).astype(BF16)
                )
                scores = jnp.where(earlier[d], scores, 0.0)
                within = jnp.dot(scores.astype(BF16), part(at, 4, h).astype(BF16), preferred_element_type=F32)
                before = states[h, d]
                carried = dot_t_state(queries * jnp.exp(cum), before)
                span = slice(h * LANES, (h + 1) * LANES)
                rec_sum[at, span] = rec_sum[at, span] + within + carried
                states[h, d] = before * jnp.exp(last) + adds[h, d, index]
        return carry

    def dot_t_state(reads, state):
        return dot_t(reads.astype(BF16), state.astype(BF16))

    lax.fori_loop(0, block_count, second_pass, 0, unroll=2)

    for h in range(heads):
        span = slice(h * LANES, (h + 1) * LANES)
        out[slot, :, span] = rms_scale(rec_sum[own_rows, span], rec_gain[...]).astype(BF16)
        if groups > 1:
            back[:, span] = rms_scale(rec_sum[other_rows, span], rec_gain[...]).astype(BF16)

    def back_copy(which):
        columns = slice(which * width, (which + 1) * width)
        return pltpu.make_async_remote_copy(
            src_ref=back.at[:, columns],
            dst_ref=out.at[slot, :, columns],
            send_sem=back_send.at[which],
            recv_sem=back_recv.at[which],
            device_id={"sp": partner},
        )

    if groups > 1:
        back_copy(0).start()

    def next_block(turn, carry):
        near = lax.div(turn + 1, 2)
        away = jnp.where(lax.rem(turn, 2) == 1, near, blocks - near)
        block = lax.rem(mine + away, blocks)
        for piece in range(groups):
            arrival(block, piece).wait_recv()
        attend(block)
        return carry

    lax.fori_loop(1, blocks, next_block, 0)

    def finish(first_row, count, store):
        for h in range(heads):
            span = slice(width + h * LANES, width + (h + 1) * LANES)
            for t in range(count):
                index = first_row + t
                ratio = mixed[h, index] / total[h, index][:, :1]
                values = ratio[:tile] - lam[h] * ratio[tile:]
                store(slice(t * tile, (t + 1) * tile), span, rms_scale(values, att_gain[...]).astype(BF16))

    part_tiles = length // tile
    if groups > 1:
        def store_back(at, span, value):
            back[at, span] = value

        finish(partner_slot * part_tiles, part_tiles, store_back)
        back_copy(1).start()

    def store_own(at, span, value):
        out[slot, at, span] = value

    finish(slot * part_tiles, part_tiles, store_own)

    for copy in own_copies + other_copies + state_copies:
        copy.wait_send()
    if groups > 1:
        swap_kv.wait_send()
        swap_rest.wait_send()
        for which in range(2):
            back_copy(which).wait()


def on_device(
    tokens, norm_gain, rec_query, fwd_gate, bwd_gate, rec_value, gate_leak, log_decay, rec_gain,
    att_query, att_key, att_value, lambdas, att_gain, out_rec, out_att,
):
    ranks = lax.axis_size("sp")
    tp = lax.axis_size("tp")
    local_heads = rec_query.shape[1] // HK
    groups = 2 if local_heads % 2 == 0 and ranks % 2 == 0 else 1
    heads = local_heads // groups
    width = heads * LANES
    slot = lax.axis_index("sp") % groups

    normed = rms_scale(tokens.astype(F32), norm_gain).astype(BF16)
    order = (att_key, att_value, att_query, rec_query, fwd_gate, bwd_gate, rec_value)
    gathered = lax.all_gather(normed, "tp", axis=0, tiled=True)
    length = gathered.shape[0]
    pieces = []
    for g in range(groups):
        for weight in order:
            pieces.append(weight[:, g * width : (g + 1) * width])
    joined = jnp.concatenate(pieces, axis=1)
    projected = jnp.dot(gathered, joined, preferred_element_type=F32).astype(BF16)
    group_width = len(order) * width
    projected = jnp.stack([projected[:, g * group_width : (g + 1) * group_width] for g in range(groups)])

    positions = (lax.axis_index("sp") * length + jnp.arange(length, dtype=jnp.int32)).astype(F32)
    frequency = THETA ** (-(jnp.arange(AK // 2, dtype=F32) * 2.0 / AK))
    angles = jnp.tile(positions[:, None] * frequency[None, :], (1, LANES // (AK // 2)))
    cosine, sine = jnp.cos(angles), jnp.sin(angles)

    by_head = log_decay.reshape(2, length, groups, heads).transpose(2, 1, 0, 3).reshape(groups, length, 2 * heads)
    own_decay = lax.dynamic_index_in_dim(by_head, slot, 0, keepdims=False)
    if groups > 1:
        swapped = lax.ppermute(
            lax.dynamic_index_in_dim(by_head, groups - 1 - slot, 0, keepdims=False),
            "sp",
            [(i, i + 1 - 2 * (i % 2)) for i in range(ranks)],
        )
        decay = jnp.where(
            slot == 0, jnp.concatenate([own_decay, swapped]), jnp.concatenate([swapped, own_decay])
        )
    else:
        decay = own_decay
    leak = lax.dynamic_index_in_dim(
        gate_leak.reshape(2, groups, heads, HK).transpose(1, 2, 0, 3), slot, 0, keepdims=False
    )
    lam = lax.dynamic_index_in_dim(lambdas.reshape(groups, heads), slot, 0, keepdims=False)
    lam = jnp.broadcast_to(lam[:, None, None], (heads, 1, LANES))

    blocks = ranks // groups
    rows = groups * length
    tile = min(256, length)
    vmem = pl.BlockSpec(memory_space=pltpu.VMEM)
    dma = pltpu.SemaphoreType.DMA
    mixers = pl.pallas_call(
        functools.partial(mixer_kernel, ranks, groups, heads, tile),
        out_shape=jax.ShapeDtypeStruct((groups, length, 2 * width), BF16),
        in_specs=[vmem] * 8,
        out_specs=vmem,
        scratch_shapes=[
            pltpu.VMEM((blocks, rows, 2 * width), BF16),
            pltpu.VMEM((rows, 5 * width), BF16),
            pltpu.VMEM((length, 7 * width), BF16),
            pltpu.VMEM((length, 2 * width), BF16),
            pltpu.VMEM((2, heads, LANES + PAD, LANES), BF16),
            pltpu.VMEM((blocks, heads, LANES + PAD, LANES), BF16),
            pltpu.VMEM((heads, 2, rows, LANES), F32),
            pltpu.VMEM((heads, 2, rows // BLOCK, LANES, LANES), F32),
            pltpu.VMEM((heads, 2, LANES, LANES), F32),
            pltpu.VMEM((rows, width), F32),
            pltpu.VMEM((heads, rows // tile, 2 * tile, LANES), F32),
            pltpu.VMEM((heads, rows // tile, 2 * tile, LANES), F32),
            pltpu.VMEM((heads, rows // tile, 2 * tile, LANES), F32),
            dma((blocks, groups)),
            dma((blocks, groups)),
            dma((2,)),
            dma,
            dma((blocks,)),
            dma((blocks,)),
            dma((2,)),
            dma((2,)),
        ],
        compiler_params=pltpu.CompilerParams(
            collective_id=0, has_side_effects=True, vmem_limit_bytes=56 * 1024 * 1024
        ),
        cost_estimate=pl.CostEstimate(flops=10**10, bytes_accessed=10**7, transcendentals=10**7),
    )(projected, cosine, sine, leak, decay, lam, rec_gain.reshape(1, LANES), att_gain.reshape(1, LANES))

    shares = mixers.reshape(groups, tp, length // tp, 2, heads, LANES)
    shares = lax.all_to_all(shares, "tp", split_axis=1, concat_axis=1)
    both = shares.transpose(2, 3, 1, 0, 4, 5).reshape(length // tp, 2, -1)
    result = jnp.dot(both[:, 0], out_rec, preferred_element_type=F32) + jnp.dot(
        both[:, 1], out_att, preferred_element_type=F32
    )
    return result.astype(BF16)


def solution(mesh):
    placed = (
        P(("sp", "tp"), None), P(), P(None, "tp"), P(None, "tp"), P(None, "tp"), P(None, "tp"),
        P(None, "tp"), P(None, "sp", "tp"), P(), P(None, "tp"), P(None, "tp"), P(None, "tp"),
        P("tp"), P(), P(), P(),
    )
    return jax.shard_map(
        on_device, mesh=mesh, in_specs=placed, out_specs=P(("sp", "tp"), None), check_vma=False
    )
```

time: 312 us -> 159 us (0.51)
  Pallas kernels: 0 us -> 87.1 us
  waiting for transfers between devices: 65.5 us -> 5.95 us
  other arithmetic: 62.4 us -> 5.92 us
  starting transfers between devices: 56.8 us -> 3.07 us
  local copies, waits for them, and re-layouts: 59.9 us -> 19.5 us
  matrix products: 49.2 us -> 12.1 us
  blocking collectives: 0 us -> 11.5 us
    pallas_call x0 -> x1, Pallas kernels: none -> 87.1 us  [on_device(): pl.pallas_call(functools.partial(mixer_kernel, ranks, groups, heads, tile...]
    ppermute x28 -> x1, waiting for transfers between devices: 46.7 us -> 0.01 us  [on_device(): lax.ppermute(lax.dynamic_index_in_dim(by_head, groups - 1 - slot, 0, keep...]
    ppermute x28 -> x1, starting transfers between devices: 49.3 us -> 3.03 us  [on_device(): lax.ppermute(lax.dynamic_index_in_dim(by_head, groups - 1 - slot, 0, keep...]
    dot_general x29 -> x3, matrix products: 49.2 us -> 12.1 us  [the longest x1 7.67 us: on_device(): jnp.dot(gathered, joined, preferred_element_type=F32).astype(BF16)]
    convert_element_type x33 -> x1, other arithmetic: 20.3 us -> 2.03 us  [on_device(): normed = rms_scale(tokens.astype(F32), norm_gain).astype(BF16)]
    add x25 -> x0, other arithmetic: 17.9 us -> none  [the longest x16 16.3 us: advance(): return (factor[..., None] * running + added_state, running)]
    while x49 -> x0, local copies, waits for them, and re-layouts: 13 us -> none
    all_to_all x0 -> x1, blocking collectives: none -> 11.5 us  [on_device(): shares = lax.all_to_all(shares, 'tp', split_axis=1, concat_axis=1)]
  transfers between devices with their start and end apart: 31 -> 2, of which waited for: 15 -> 1; matrix products, arithmetic and copies ran while one was open for 19% -> 11% of each run, Pallas kernels for 0% -> 0%
where the time goes in v1:
time: 159 us
  Pallas kernels  87.1 us (55%)
  local copies, waits for them, and re-layouts  19.5 us (12%)
  between operations  13.7 us (9%)
  matrix products  12.1 us (8%)
  blocking collectives  11.5 us (7%)
  waiting for transfers between devices  5.95 us (4%)
  other arithmetic  5.92 us (4%)
  starting transfers between devices  3.07 us (2%)
    pallas_call x1, Pallas kernels, on_device(): pl.pallas_call(functools.partial(mixer_kernel, ranks, groups, heads, tile...  87.1 us
    unnamed x37, local copies, waits for them, and re-layouts  12.2 us
    all_to_all x1, blocking collectives, on_device(): shares = lax.all_to_all(shares, 'tp', split_axis=1, concat_axis=1)  11.5 us
    dot_general x1, matrix products, on_device(): jnp.dot(gathered, joined, preferred_element_type=F32).astype(BF16)  7.67 us
    all_gather x1, waiting for transfers between devices, on_device(): gathered = lax.all_gather(normed, 'tp', axis=0, tiled=True)  5.93 us
  transfers between devices with their start and end apart: 2, of which 1 were waited for; matrix products, arithmetic and copies ran while one was open for 11% of the time, Pallas kernels for 0%

profile of v1, /device:TPU:0, one launch (start us, length us, event | category | flops | bytes accessed | tf_op | source)
XLA Modules:
  0.0 158.9 jit_solution(11289814803142367747)
XLA Ops:
  6.5 0.0 copy-start
  6.5 0.0 copy-start.2
  6.5 0.0 copy-start.3
  6.5 0.0 copy-start.4
  6.5 0.0 all-gather.2.cloned.1.call-start
  6.6 0.9 constant_dynamic-slice_fusion.1
  7.5 3.0 %collective-permute-start = (f32[512,2]{0,1:T(2,128)S(1)}, f32[512,2]{0,1:T(2,128)S(1)}, u32[]{:S(2)}, u32[]{:S(2)}) collective-permute-start(f32[512,2]{0,1:T(2,128)S(1)} %bitcast.47), channel_id=1, source_target_pairs={{0,4},{4,0},{8,12},{12,8},{16,20},{20,16},{24,28},{28,24},{1,5},{5... | collective-permute-start | bytes 12296 | tf_op jit(solution)/shard_map/ppermute | solution.py:376
  10.5 1.2 fusion.1
  11.8 2.0 %fusion.3 = bf16[128,2048]{1,0:T(8,128)(2,1)} fusion(bf16[128,2048]{1,0:T(8,128)(2,1)} %param.16, f32[2048]{0:T(1024)} %param.17, f32[128]{0:T(128)S(1)} %add_rsqrt_fusion), kind=kLoop, calls=%fused_computation.8 | loop fusion | flops 1048576 | bytes 1057280 | tf_op jit(solution)/shard_map/convert_element_type | solution.py:355
  13.8 0.0 all-gather.2.cloned.1.call-update
  13.8 0.0 copy-start.5
  13.8 0.0 copy-start.6
  13.9 0.0 copy-start.7
  13.9 0.0 copy-start.8
  13.9 0.0 copy-start.10
  13.9 1.3 slice_dynamic-update-slice_fusion.13
  15.2 1.2 slice_dynamic-update-slice_fusion.12
  16.4 1.2 slice_dynamic-update-slice_fusion.11
  17.6 1.2 slice_dynamic-update-slice_fusion.10
  18.8 1.2 slice_dynamic-update-slice_fusion.9
  19.9 1.2 slice_dynamic-update-slice_fusion.8
  21.1 1.2 slice_dynamic-update-slice_fusion.7
  22.3 0.0 copy-done.2
  22.4 0.1 slice_dynamic-update-slice_fusion.6
  22.5 0.0 copy-done.3
  22.5 0.1 slice_dynamic-update-slice_fusion.5
  22.6 0.3 multiply_sine_fusion
  23.0 0.0 copy-done.4
  23.0 0.1 slice_dynamic-update-slice_fusion.4
  23.1 0.0 copy-done.5
  23.1 0.1 slice_dynamic-update-slice_fusion.3
  23.2 0.0 copy-done.6
  23.3 0.1 slice_dynamic-update-slice_fusion.2
  23.4 0.0 copy-done.7
  23.4 0.1 slice_dynamic-update-slice_fusion.1
  23.5 0.0 copy-done.8
  23.5 0.1 slice_dynamic-update-slice_fusion
  23.7 0.0 copy-start.9
  23.7 2.9 %copy-done.9 = bf16[2048,1792]{1,0:T(8,128)(2,1)} copy-done((bf16[2048,1792]{1,0:T(8,128)(2,1)}, bf16[2048,1792]{1,0:T(8,128)(2,1)S(1)}, u32[]{:S(2)}) %copy-start.9) | copy-done | bytes 7340056
  26.6 0.0 copy-done
  26.6 0.6 dynamic-slice_bitcast_fusion.leak
  27.2 0.0 copy-done.10
  27.2 0.6 dynamic-slice.19
  27.8 0.8 copy.40.cosine
  28.7 0.9 copy.41.sine
  29.6 0.0 collective-permute-done
  29.6 0.2 copy.38
  29.8 0.2 copy.39
  30.1 0.9 broadcast_select_fusion.decay
  30.9 5.9 %all-gather.2.cloned.1.call-done = bf16[512,2048]{1,0:T(8,128)(2,1)} async-done(((bf16[128,2048]{1,0:T(8,128)(2,1)}), bf16[512,2048]{1,0:T(8,128)(2,1)}) %all-gather.2.cloned.1.call-update) | async-done | bytes 2097168 | tf_op jit(solution)/shard_map/all_gather | solution.py:357
  36.9 7.7 %convolution_convert_fusion = bf16[512,1792]{1,0:T(8,128)(2,1)S(1)} fusion(bf16[512,2048]{1,0:T(8,128)(2,1)} %all-gather.2.cloned.1.call-done, bf16[2048,1792]{1,0:T(8,128)(2,1)} %copy-done.9), kind=kOutput, calls=%fused_computation | convolution fusion | flops 3759013888 | bytes 11272192 | tf_op jit(solution)/shard_map/dot_general | solution.py:364
  44.5 0.1 slice_bitcast_fusion.1
  44.7 1.5 pad_maximum_fusion.proj
  46.2 1.1 broadcast_in_dim.5.lam
  47.3 87.1 %shard_map.154 = bf16[2,512,256]{2,1,0:T(8,128)(2,1)} custom-call(bf16[2,512,896]{2,1,0:T(8,128)(2,1)} %pad_maximum_fusion.proj, f32[512,128]{1,0:T(8,128)} %copy.40.cosine, f32[512,128]{1,0:T(8,128)} %copy.41.sine, f32[1,2,128]{2,1,0:T(2,128)} %dynamic-slice_bitcast_fusion.leak, f32[1024,2]{1,0:T(8,128)} %broadcast_select_fusion.decay, ...), custom_call_target="tpu_custom_call" | custom-call | flops 10000000000 | bytes 10000000 | tf_op jit(solution)/shard_map/pallas_call | solution.py:397
  134.4 1.2 reshape.92
  135.5 0.4 copy.42
  136.0 0.0 copy-start.1
  136.0 11.5 %all_to_all.5 = bf16[2,4,128,2,1,128]{2,5,0,3,4,1:T(8,128)(2,1)S(1)} all-to-all(bf16[2,4,128,2,1,128]{2,5,0,3,4,1:T(8,128)(2,1)S(1)} %copy.42), channel_id=1, replica_groups=mesh['sp'=8,'tp'=4] {'tp'}, dimensions={1} | all-to-all | bytes 1048576 | tf_op jit(solution)/shard_map/all_to_all | solution.py:432
  147.5 2.9 %fusion.4 = f32[128,2048]{1,0:T(8,128)S(1)} fusion(bf16[1024,2048]{1,0:T(8,128)(2,1)} %param.30, bf16[128,2,1024]{0,2,1:T(8,128)(2,1)S(1)} %bitcast.42), kind=kOutput, calls=%fused_computation.27 | convolution fusion | flops 536870912 | bytes 5505024 | tf_op jit(solution)/shard_map/dot_general | solution.py:434
  150.5 0.0 copy-done.1
  150.5 1.5 fusion
  (9 shorter events, 0.1 us)
Async XLA Ops:
  6.5 20.1 %copy-start = (f32[2,256]{1,0:T(2,128)S(1)}, f32[2,256]{1,0:T(2,128)}, u32[]{:S(2)}) copy-start(f32[2,256]{1,0:T(2,128)} %param.22) | copy-start | bytes 6148
  6.5 15.8 %copy-start.2 = (bf16[2048,256]{1,0:T(8,128)(2,1)S(1)}, bf16[2048,256]{1,0:T(8,128)(2,1)}, u32[]{:S(2)}) copy-start(bf16[2048,256]{1,0:T(8,128)(2,1)} %param.26) | copy-start | bytes 3145732
  6.5 15.9 %copy-start.3 = (bf16[2048,256]{1,0:T(8,128)(2,1)S(1)}, bf16[2048,256]{1,0:T(8,128)(2,1)}, u32[]{:S(2)}) copy-start(bf16[2048,256]{1,0:T(8,128)(2,1)} %param.27) | copy-start | bytes 3145732
  6.5 16.4 %copy-start.4 = (bf16[2048,256]{1,0:T(8,128)(2,1)S(1)}, bf16[2048,256]{1,0:T(8,128)(2,1)}, u32[]{:S(2)}) copy-start(bf16[2048,256]{1,0:T(8,128)(2,1)} %param.25) | copy-start | bytes 3145732
  6.5 30.3 %all-gather.2.cloned.1.call-start = ((), (), s32[]{:S(2)}) async-start(), calls=%async_computation.1 | async-start | bytes 2621440 | tf_op jit(solution)/shard_map/all_gather | solution.py:357
  7.5 22.1 %collective-permute-start = (f32[512,2]{0,1:T(2,128)S(1)}, f32[512,2]{0,1:T(2,128)S(1)}, u32[]{:S(2)}, u32[]{:S(2)}) collective-permute-start(f32[512,2]{0,1:T(2,128)S(1)} %bitcast.47), channel_id=1, source_target_pairs={{0,4},{4,0},{8,12},{12,8},{16,20},{20,16},{24,28},{28,24},{1,5},{5... | collective-permute-start | bytes 12296 | tf_op jit(solution)/shard_map/ppermute | solution.py:376
  13.8 9.3 %copy-start.5 = (bf16[2048,256]{1,0:T(8,128)(2,1)S(1)}, bf16[2048,256]{1,0:T(8,128)(2,1)}, u32[]{:S(2)}) copy-start(bf16[2048,256]{1,0:T(8,128)(2,1)} %param.18) | copy-start | bytes 3145732
  13.8 9.4 %copy-start.6 = (bf16[2048,256]{1,0:T(8,128)(2,1)S(1)}, bf16[2048,256]{1,0:T(8,128)(2,1)}, u32[]{:S(2)}) copy-start(bf16[2048,256]{1,0:T(8,128)(2,1)} %param.19) | copy-start | bytes 3145732
  13.9 9.5 %copy-start.7 = (bf16[2048,256]{1,0:T(8,128)(2,1)S(1)}, bf16[2048,256]{1,0:T(8,128)(2,1)}, u32[]{:S(2)}) copy-start(bf16[2048,256]{1,0:T(8,128)(2,1)} %param.20) | copy-start | bytes 3145732
  13.9 9.7 %copy-start.8 = (bf16[2048,256]{1,0:T(8,128)(2,1)S(1)}, bf16[2048,256]{1,0:T(8,128)(2,1)}, u32[]{:S(2)}) copy-start(bf16[2048,256]{1,0:T(8,128)(2,1)} %param.21) | copy-start | bytes 3145732
  13.9 13.3 %copy-start.10 = (f32[2]{0:T(128)S(1)}, f32[2]{0:T(128)}, u32[]{:S(2)}) copy-start(f32[2]{0:T(128)} %param.28) | copy-start | bytes 28
  23.7 2.9 %copy-start.9 = (bf16[2048,1792]{1,0:T(8,128)(2,1)}, bf16[2048,1792]{1,0:T(8,128)(2,1)S(1)}, u32[]{:S(2)}) copy-start(bf16[2048,1792]{1,0:T(8,128)(2,1)S(1)} %slice_dynamic-update-slice_fusion) | copy-start | bytes 22020100
  136.0 14.5 %copy-start.1 = (bf16[1024,2048]{1,0:T(8,128)(2,1)S(1)}, bf16[1024,2048]{1,0:T(8,128)(2,1)}, u32[]{:S(2)}) copy-start(bf16[1024,2048]{1,0:T(8,128)(2,1)} %param.31) | copy-start | bytes 12582916
Sparse Core Ops, SparseCore 0:
  13.9 22.8 all-gather.1

commit v2 on v1

--- a/solution.py
+++ b/solution.py
@@ -31,17 +31,84 @@
     return lax.dot_general(a, b, (((0,), (0,)), ((), ())), preferred_element_type=F32)
 
 
+def gather_kernel(tp, tokens, gain, *refs):
+    weights, outs = refs[:7], refs[7:14]
+    held, across, along, landed = refs[14:]
+    me = lax.axis_index("tp")
+    core = lax.rem(me, 2)
+    pair = lax.div(me, 2)
+    pairs = tp // 2
+    count = tokens.shape[0]
+    partner = pair * 2 + 1 - core
+    others = [lax.rem(pair + k, pairs) for k in range(1, pairs)]
+    barrier = pltpu.get_barrier_semaphore()
+    pl.semaphore_signal(barrier, inc=1, device_id={"tp": partner})
+    for q in others:
+        pl.semaphore_signal(barrier, inc=1, device_id={"tp": q * 2 + core})
+
+    def rows_at(block):
+        return held.at[pl.ds(pl.multiple_of(block * count, count), count)]
+
+    def to_partner(block):
+        return pltpu.make_async_remote_copy(
+            src_ref=rows_at(block),
+            dst_ref=rows_at(block),
+            send_sem=across.at[block],
+            recv_sem=landed.at[block],
+            device_id={"tp": partner},
+        )
+
+    def to_pair(q):
+        return pltpu.make_async_remote_copy(
+            src_ref=rows_at(me),
+            dst_ref=rows_at(me),
+            send_sem=along.at[q],
+            recv_sem=landed.at[me],
+            device_id={"tp": q * 2 + core},
+        )
+
+    normed = rms_scale(tokens[...].astype(F32), gain[...]).astype(BF16)
+    held[pl.ds(pl.multiple_of(me * count, count), count), :] = normed
+    pl.semaphore_wait(barrier, pairs)
+    for q in others:
+        to_pair(q).start()
+    to_partner(me).start()
+
+    def step(k, carry):
+        q = lax.rem(pair + k, pairs)
+        near = q * 2 + core
+
+        @pl.when(k > 0)
+        def _():
+            to_partner(near).wait_recv()
+            to_partner(near).start()
+
+        to_partner(q * 2 + 1 - core).wait_recv()
+        at = pl.ds(pl.multiple_of(q * 2 * count, 2 * count), 2 * count)
+        for weight, result in zip(weights, outs):
+            result[at, :] = jnp.dot(held[at, :], weight[...], preferred_element_type=F32).astype(BF16)
+        return carry
+
+    lax.fori_loop(0, pairs, step, 0)
+    to_partner(me).wait_send()
+    for q in others:
+        to_pair(q).wait_send()
+        to_partner(q * 2 + core).wait_send()
+
+
 def mixer_kernel(
-    ranks, groups, heads, tile,
-    proj, cosine, sine, leak, decay, lam, rec_gain, att_gain,
+    ranks, tp, groups, heads, tile,
+    proj_k, proj_v, proj_q, proj_rq, proj_fwd, proj_bwd, proj_rv, cosine, sine, leak, decay, lam, rec_gain, att_gain,
     out,
-    kv, rest, swap, back, state_out, state_in, cums, adds, states, rec_sum, peak, total, mixed,
-    kv_send, kv_recv, swap_send, rest_recv, state_send, state_recv, back_send, back_recv,
+    kv, rest, swap, stage, state_out, state_in, cums, adds, states, rec_sum, peak, total, mixed,
+    kv_send, kv_recv, swap_send, rest_recv, state_send, state_recv, out_send, out_recv,
 ):
     me = lax.axis_index("sp")
     slot = lax.rem(me, groups)
     mine = lax.div(me, groups)
-    length = proj.shape[1]
+    mesh_column = lax.axis_index("tp")
+    length = proj_k.shape[0]
+    piece = length // tp
     rows = groups * length
     width = heads * LANES
     block_count = rows // BLOCK
@@ -57,8 +124,12 @@
         peers.append(lax.rem(mine + k, blocks))
     for peer in peers:
         pl.semaphore_signal(barrier, inc=1, device_id={"sp": peer * groups + slot})
-    if groups > 1:
-        pl.semaphore_signal(barrier, inc=1, device_id={"sp": partner})
+    owners = []
+    for dp in range(groups):
+        for dt in range(tp):
+            owners.append((dp, dt, lax.rem(slot + dp, groups), lax.rem(mesh_column + dt, tp)))
+    for dp, dt, p, t in owners[1:]:
+        pl.semaphore_signal(barrier, inc=1, device_id={"sp": mine * groups + p, "tp": t})
 
     lane = lax.broadcasted_iota(jnp.int32, (length, LANES), 1)
     low_half = lax.rem(lane, AK) < AK // 2
@@ -69,21 +140,21 @@
         return wide * cosine[...] + turned * sine[...]
 
     def prepare(head_group, key_value, others):
+        def taken(ref, h):
+            return ref[:, pl.ds(pl.multiple_of((head_group * heads + h) * LANES, LANES), LANES)]
+
         for h in range(heads):
             at = h * LANES
-            key_value[:, at : at + LANES] = rotated(proj[head_group, :, at : at + LANES]).astype(BF16)
-        key_value[:, width : 2 * width] = proj[head_group, :, width : 2 * width]
-        for h in range(heads):
-            at = 2 * width + h * LANES
-            others[:, h * LANES : (h + 1) * LANES] = (
-                rotated(proj[head_group, :, at : at + LANES]) * AK ** (-0.5)
-            ).astype(BF16)
-        others[:, width:] = proj[head_group, :, 3 * width :]
+            key_value[:, at : at + LANES] = rotated(taken(proj_k, h)).astype(BF16)
+            key_value[:, width + at : width + at + LANES] = taken(proj_v, h)
+            others[:, at : at + LANES] = (rotated(taken(proj_q, h)) * AK ** (-0.5)).astype(BF16)
+            for i, ref in enumerate((proj_rq, proj_fwd, proj_bwd, proj_rv)):
+                others[:, (i + 1) * width + at : (i + 1) * width + at + LANES] = taken(ref, h)
 
     if groups > 1:
         prepare(partner_slot, swap.at[:, : 2 * width], swap.at[:, 2 * width :])
     prepare(slot, kv.at[mine, own_rows], rest.at[own_rows])
-    pl.semaphore_wait(barrier, blocks - 1 + (groups - 1))
+    pl.semaphore_wait(barrier, blocks - 1 + groups * tp - 1)
 
     def block_copy(source_rows, source_slot, peer):
         return pltpu.make_async_remote_copy(
@@ -281,22 +352,37 @@
 
     for h in range(heads):
         span = slice(h * LANES, (h + 1) * LANES)
-        out[slot, :, span] = rms_scale(rec_sum[own_rows, span], rec_gain[...]).astype(BF16)
-        if groups > 1:
-            back[:, span] = rms_scale(rec_sum[other_rows, span], rec_gain[...]).astype(BF16)
-
-    def back_copy(which):
+        stage[:, span] = rms_scale(rec_sum[:, span], rec_gain[...]).astype(BF16)
+
+    def hand_over(which, owner):
+        dp, dt, p, t = owner
         columns = slice(which * width, (which + 1) * width)
-        return pltpu.make_async_remote_copy(
-            src_ref=back.at[:, columns],
-            dst_ref=out.at[slot, :, columns],
-            send_sem=back_send.at[which],
-            recv_sem=back_recv.at[which],
-            device_id={"sp": partner},
-        )
-
-    if groups > 1:
-        back_copy(0).start()
+        source = stage.at[pl.ds(pl.multiple_of(p * length + t * piece, piece), piece), columns]
+        target = out.at[mesh_column, slot, :, columns]
+        if dp == 0 and dt == 0:
+            return pltpu.make_async_copy(source, target, out_send.at[which, dp, dt])
+        return pltpu.make_async_remote_copy(
+            src_ref=source,
+            dst_ref=target,
+            send_sem=out_send.at[which, dp, dt],
+            recv_sem=out_recv.at[which, mesh_column, slot],
+            device_id={"sp": mine * groups + p, "tp": t},
+        )
+
+    def taken_over(which, owner):
+        dp, dt, p, t = owner
+        columns = slice(which * width, (which + 1) * width)
+        target = out.at[t, p, :, columns]
+        return pltpu.make_async_remote_copy(
+            src_ref=target,
+            dst_ref=target,
+            send_sem=out_send.at[which, dp, dt],
+            recv_sem=out_recv.at[which, t, p],
+            device_id={"sp": mine * groups + p, "tp": t},
+        )
+
+    for owner in owners:
+        hand_over(0, owner).start()
 
     def next_block(turn, carry):
         near = lax.div(turn + 1, 2)
@@ -309,35 +395,25 @@
 
     lax.fori_loop(1, blocks, next_block, 0)
 
-    def finish(first_row, count, store):
-        for h in range(heads):
-            span = slice(width + h * LANES, width + (h + 1) * LANES)
-            for t in range(count):
-                index = first_row + t
-                ratio = mixed[h, index] / total[h, index][:, :1]
-                values = ratio[:tile] - lam[h] * ratio[tile:]
-                store(slice(t * tile, (t + 1) * tile), span, rms_scale(values, att_gain[...]).astype(BF16))
-
-    part_tiles = length // tile
-    if groups > 1:
-        def store_back(at, span, value):
-            back[at, span] = value
-
-        finish(partner_slot * part_tiles, part_tiles, store_back)
-        back_copy(1).start()
-
-    def store_own(at, span, value):
-        out[slot, at, span] = value
-
-    finish(slot * part_tiles, part_tiles, store_own)
+    for h in range(heads):
+        span = slice(width + h * LANES, width + (h + 1) * LANES)
+        for index in range(tiles):
+            ratio = mixed[h, index] / total[h, index][:, :1]
+            values = ratio[:tile] - lam[h] * ratio[tile:]
+            stage[index * tile : (index + 1) * tile, span] = rms_scale(values, att_gain[...]).astype(BF16)
+    for owner in owners:
+        hand_over(1, owner).start()
 
     for copy in own_copies + other_copies + state_copies:
         copy.wait_send()
     if groups > 1:
         swap_kv.wait_send()
         swap_rest.wait_send()
-        for which in range(2):
-            back_copy(which).wait()
+    for which in range(2):
+        hand_over(which, owners[0]).wait()
+        for owner in owners[1:]:
+            hand_over(which, owner).wait_send()
+            taken_over(which, owner).wait_recv()
 
 
 def on_device(
@@ -352,18 +428,26 @@
     width = heads * LANES
     slot = lax.axis_index("sp") % groups
 
-    normed = rms_scale(tokens.astype(F32), norm_gain).astype(BF16)
     order = (att_key, att_value, att_query, rec_query, fwd_gate, bwd_gate, rec_value)
-    gathered = lax.all_gather(normed, "tp", axis=0, tiled=True)
-    length = gathered.shape[0]
-    pieces = []
-    for g in range(groups):
-        for weight in order:
-            pieces.append(weight[:, g * width : (g + 1) * width])
-    joined = jnp.concatenate(pieces, axis=1)
-    projected = jnp.dot(gathered, joined, preferred_element_type=F32).astype(BF16)
-    group_width = len(order) * width
-    projected = jnp.stack([projected[:, g * group_width : (g + 1) * group_width] for g in range(groups)])
+    length = tokens.shape[0] * tp
+    vmem = pl.BlockSpec(memory_space=pltpu.VMEM)
+    dma = pltpu.SemaphoreType.DMA
+    projected = pl.pallas_call(
+        functools.partial(gather_kernel, tp),
+        out_shape=[jax.ShapeDtypeStruct((length, weight.shape[1]), BF16) for weight in order],
+        in_specs=[vmem] * (2 + len(order)),
+        out_specs=[vmem] * len(order),
+        scratch_shapes=[
+            pltpu.VMEM((length, tokens.shape[1]), BF16),
+            dma((tp,)),
+            dma((tp // 2,)),
+            dma((tp,)),
+        ],
+        compiler_params=pltpu.CompilerParams(
+            collective_id=1, has_side_effects=True, vmem_limit_bytes=40 * 1024 * 1024
+        ),
+        cost_estimate=pl.CostEstimate(flops=4 * 10**9, bytes_accessed=10**7, transcendentals=0),
+    )(tokens, norm_gain.reshape(1, -1), *order)
 
     positions = (lax.axis_index("sp") * length + jnp.arange(length, dtype=jnp.int32)).astype(F32)
     frequency = THETA ** (-(jnp.arange(AK // 2, dtype=F32) * 2.0 / AK))
@@ -392,18 +476,16 @@
     blocks = ranks // groups
     rows = groups * length
     tile = min(256, length)
-    vmem = pl.BlockSpec(memory_space=pltpu.VMEM)
-    dma = pltpu.SemaphoreType.DMA
     mixers = pl.pallas_call(
-        functools.partial(mixer_kernel, ranks, groups, heads, tile),
-        out_shape=jax.ShapeDtypeStruct((groups, length, 2 * width), BF16),
-        in_specs=[vmem] * 8,
+        functools.partial(mixer_kernel, ranks, tp, groups, heads, tile),
+        out_shape=jax.ShapeDtypeStruct((tp, groups, length // tp, 2 * width), BF16),
+        in_specs=[vmem] * 14,
         out_specs=vmem,
         scratch_shapes=[
             pltpu.VMEM((blocks, rows, 2 * width), BF16),
             pltpu.VMEM((rows, 5 * width), BF16),
             pltpu.VMEM((length, 7 * width), BF16),
-            pltpu.VMEM((length, 2 * width), BF16),
+            pltpu.VMEM((rows, 2 * width), BF16),
             pltpu.VMEM((2, heads, LANES + PAD, LANES), BF16),
             pltpu.VMEM((blocks, heads, LANES + PAD, LANES), BF16),
             pltpu.VMEM((heads, 2, rows, LANES), F32),
@@ -419,18 +501,17 @@
             dma,
             dma((blocks,)),
             dma((blocks,)),
-            dma((2,)),
-            dma((2,)),
+            dma((2, groups, tp)),
+            dma((2, tp, groups)),
         ],
         compiler_params=pltpu.CompilerParams(
             collective_id=0, has_side_effects=True, vmem_limit_bytes=56 * 1024 * 1024
         ),
         cost_estimate=pl.CostEstimate(flops=10**10, bytes_accessed=10**7, transcendentals=10**7),
-    )(projected, cosine, sine, leak, decay, lam, rec_gain.reshape(1, LANES), att_gain.reshape(1, LANES))
-
-    shares = mixers.reshape(groups, tp, length // tp, 2, heads, LANES)
-    shares = lax.all_to_all(shares, "tp", split_axis=1, concat_axis=1)
-    both = shares.transpose(2, 3, 1, 0, 4, 5).reshape(length // tp, 2, -1)
+    )(*projected, cosine, sine, leak, decay, lam, rec_gain.reshape(1, LANES), att_gain.reshape(1, LANES))
+
+    shares = mixers.reshape(tp, groups, length // tp, 2, heads, LANES)
+    both = shares.transpose(2, 3, 0, 1, 4, 5).reshape(length // tp, 2, -1)
     result = jnp.dot(both[:, 0], out_rec, preferred_element_type=F32) + jnp.dot(
         both[:, 1], out_att, preferred_element_type=F32
     )

time: 159 us -> 137 us (0.86)
  Pallas kernels: 87.1 us -> 105 us
  between operations: 13.7 us -> 0.13 us
  blocking collectives: 11.5 us -> 0 us
  matrix products: 12.1 us -> 4.62 us
  waiting for transfers between devices: 5.95 us -> 0.01 us
  other arithmetic: 5.92 us -> 1.19 us
  local copies, waits for them, and re-layouts: 19.5 us -> 22.5 us
    pallas_call x1 -> x2, Pallas kernels: 87.1 us -> 105 us  [the longest x1 88.2 us: on_device(): pl.pallas_call(functools.partial(mixer_kernel, ranks, tp, groups, heads,...]
    all_to_all x1 -> x0, blocking collectives: 11.5 us -> none  [on_device(): shares = lax.all_to_all(shares, 'tp', split_axis=1, concat_axis=1)]
    dot_general x1 -> x0, matrix products: 7.67 us -> none  [on_device(): jnp.dot(gathered, joined, preferred_element_type=F32).astype(BF16)]
    all_gather x1 -> x0, waiting for transfers between devices: 5.93 us -> none  [on_device(): gathered = lax.all_gather(normed, 'tp', axis=0, tiled=True)]
    unnamed x37 -> x40, local copies, waits for them, and re-layouts: 12.2 us -> 15.5 us
    convert_element_type x1 -> x0, other arithmetic: 2.03 us -> none  [on_device(): normed = rms_scale(tokens.astype(F32), norm_gain).astype(BF16)]
  transfers between devices with their start and end apart: 2 -> 1, of which waited for: 1 -> 0; matrix products, arithmetic and copies ran while one was open for 11% -> 2% of each run, Pallas kernels for 0% -> 12%
where the time goes in v2:
time: 137 us
  Pallas kernels  105 us (77%)
  local copies, waits for them, and re-layouts  22.5 us (16%)
  matrix products  4.62 us (3%)
  starting transfers between devices  3.03 us (2%)
    pallas_call x1, Pallas kernels, on_device(): pl.pallas_call(functools.partial(mixer_kernel, ranks, tp, groups, heads,...  88.2 us
    pallas_call x1, Pallas kernels, on_device(): pl.pallas_call(functools.partial(gather_kernel, tp), out_shape=[jax.Shape...  17.1 us
    unnamed x40, local copies, waits for them, and re-layouts  15.5 us
    dot_general x1, matrix products, on_device(): jnp.dot(both[:, 0], out_rec, preferred_element_type=F32)  3.08 us
    ppermute x1, starting transfers between devices, on_device(): lax.ppermute(lax.dynamic_index_in_dim(by_head, groups - 1 - slot, 0, keep...  3.03 us
  transfers between devices with their start and end apart: 1, of which 0 were waited for; matrix products, arithmetic and copies ran while one was open for 2% of the time, Pallas kernels for 12%

profile of v2, /device:TPU:0, one launch (start us, length us, event | category | flops | bytes accessed | tf_op | source)
XLA Modules:
  0.0 136.8 jit_solution(5077967458325571512)
XLA Ops:
  0.0 0.0 copy-start
  0.0 0.8 constant_dynamic-slice_fusion.1
  0.8 3.0 %collective-permute-start = (f32[512,2]{0,1:T(2,128)S(1)}, f32[512,2]{0,1:T(2,128)S(1)}, u32[]{:S(2)}, u32[]{:S(2)}) collective-permute-start(f32[512,2]{0,1:T(2,128)S(1)} %bitcast.45), channel_id=1, source_target_pairs={{0,4},{4,0},{8,12},{12,8},{16,20},{20,16},{24,28},{28,24},{1,5},{5... | collective-permute-start | bytes 12296 | tf_op jit(solution)/shard_map/ppermute | solution.py:460
  3.8 0.3 multiply_sine_fusion
  4.2 0.0 copy-start.1
  4.2 1.2 copy-done.1
  5.4 0.0 copy-start.2
  5.4 1.2 copy-done.2
  6.6 0.0 copy-start.3
  6.6 1.2 copy-done.3
  7.8 0.0 copy-start.4
  7.8 1.2 copy-done.4
  9.1 0.0 copy-start.5
  9.1 1.2 copy-done.5
  10.3 0.0 copy-start.6
  10.3 1.2 copy-done.6
  11.5 0.0 copy-start.7
  11.5 1.2 copy-done.7
  12.7 0.0 copy-start.8
  12.7 1.0 copy-done.8
  13.8 0.0 copy-start.9
  13.8 0.7 copy-done.9
  14.5 0.0 copy-start.18
  14.5 17.1 %shard_map.154 = (bf16[512,256]{1,0:T(8,128)(2,1)S(1)}, bf16[512,256]{1,0:T(8,128)(2,1)S(1)}, bf16[512,256]{1,0:T(8,128)(2,1)S(1)}, bf16[512,256]{1,0:T(8,128)(2...) custom-call(bf16[128,2048]{1,0:T(8,128)(2,1)S(1)} %copy-done.8, ...), custom_call_target="tpu_custom_call" | custom-call | flops 4000000000 | bytes 10000000 | tf_op jit(solution)/shard_map/pallas_call | solution.py:435
  31.6 0.0 copy-start.10
  31.6 0.7 copy-done.10
  32.3 0.0 copy-start.11
  32.3 0.7 copy-done.11
  33.0 0.0 copy-start.12
  33.0 0.7 copy-done.12
  33.7 0.0 copy-start.13
  33.7 0.7 copy-done.13
  34.4 0.0 copy-start.14
  34.4 0.7 copy-done.14
  35.1 0.0 copy-start.15
  35.1 0.7 copy-done.15
  35.7 0.0 copy-start.16
  35.8 0.7 copy-done.16
  36.5 0.0 copy-done
  36.5 0.5 dynamic-slice_bitcast_fusion.leak
  37.0 0.0 copy-done.18
  37.0 0.6 dynamic-slice.19
  37.7 0.8 copy.40.sine
  38.5 0.8 copy.39.cosine
  39.4 0.0 collective-permute-done
  39.4 0.2 copy.38
  39.6 0.2 copy.37
  39.9 0.9 broadcast_select_fusion.decay
  40.7 1.2 broadcast_in_dim.5.lam
  41.9 88.2 %shard_map.155 = bf16[4,2,128,256]{3,2,1,0:T(8,128)(2,1)} custom-call(bf16[512,256]{1,0:T(8,128)(2,1)} %copy-done.10, bf16[512,256]{1,0:T(8,128)(2,1)} %copy-done.11, bf16[512,256]{1,0:T(8,128)(2,1)} %copy-done.12, bf16[512,256]{1,0:T(8,128)(2,1)} %copy-done.13, bf16[512,256]{1,0:T(8,128)(2,1)} %copy-done.14, bf16[512,256]{1,0:T(8,128)(2,1)} %copy-done.15, ...), custom_call_target="tpu_custom_call" | custom-call | flops 10000000000 | bytes 10000000 | tf_op jit(solution)/shard_map/pallas_call | solution.py:479
  130.1 1.2 reshape.87
  131.3 0.5 copy.41
  131.8 0.0 copy-start.17
  131.8 3.1 %fusion.1 = f32[128,2048]{1,0:T(8,128)S(1)} fusion(bf16[1024,2048]{1,0:T(8,128)(2,1)} %param.30, bf16[128,2,1024]{0,2,1:T(8,128)(2,1)S(1)} %bitcast.40), kind=kOutput, calls=%fused_computation.4 | convolution fusion | flops 536870912 | bytes 5505024 | tf_op jit(solution)/shard_map/dot_general | solution.py:515
  134.9 0.4 copy-done.17
  135.2 1.5 %fusion = bf16[128,2048]{1,0:T(8,128)(2,1)} fusion(f32[128,2048]{1,0:T(8,128)S(1)} %fusion.1, bf16[1024,2048]{1,0:T(8,128)(2,1)S(1)} %copy-done.17, bf16[128,2,1024]{0,2,1:T(8,128)(2,1)S(1)} %bitcast.41), kind=kOutput, calls=%fused_computation.1 | convolution fusion | flops 537395200 | bytes 6029312 | tf_op jit(solution)/shard_map/dot_general | solution.py:515
  (7 shorter events, 0.1 us)
Async XLA Ops:
  0.0 36.5 %copy-start = (f32[2,256]{1,0:T(2,128)S(1)}, f32[2,256]{1,0:T(2,128)}, u32[]{:S(2)}) copy-start(f32[2,256]{1,0:T(2,128)} %param.22) | copy-start | bytes 6148
  0.8 38.6 %collective-permute-start = (f32[512,2]{0,1:T(2,128)S(1)}, f32[512,2]{0,1:T(2,128)S(1)}, u32[]{:S(2)}, u32[]{:S(2)}) collective-permute-start(f32[512,2]{0,1:T(2,128)S(1)} %bitcast.45), channel_id=1, source_target_pairs={{0,4},{4,0},{8,12},{12,8},{16,20},{20,16},{24,28},{28,24},{1,5},{5... | collective-permute-start | bytes 12296 | tf_op jit(solution)/shard_map/ppermute | solution.py:460
  4.2 1.2 copy-start.1
  5.4 1.2 copy-start.2
  6.6 1.2 copy-start.3
  7.8 1.2 copy-start.4
  9.1 1.2 copy-start.5
  10.3 1.2 copy-start.6
  11.5 1.2 copy-start.7
  12.7 1.0 copy-start.8
  13.8 0.7 copy-start.9
  14.5 22.5 %copy-start.18 = (f32[2]{0:T(128)S(1)}, f32[2]{0:T(128)}, u32[]{:S(2)}) copy-start(f32[2]{0:T(128)} %param.28) | copy-start | bytes 28
  31.6 0.7 copy-start.10
  32.3 0.7 copy-start.11
  33.0 0.7 copy-start.12
  33.7 0.7 copy-start.13
  34.4 0.7 copy-start.14
  35.1 0.7 copy-start.15
  35.7 0.7 copy-start.16
  131.8 3.5 %copy-start.17 = (bf16[1024,2048]{1,0:T(8,128)(2,1)S(1)}, bf16[1024,2048]{1,0:T(8,128)(2,1)}, u32[]{:S(2)}) copy-start(bf16[1024,2048]{1,0:T(8,128)(2,1)} %param.31) | copy-start | bytes 12582916
